TPU v7x, 32 devices: a whole 2x2x4 slice. The times are simulated.
32 devices in a mesh: tp: 16 (over z, y, x), dp: 2 (over core).
Axes of the slice: x: 2, y: 2, z: 4, core: 2. Of those that a mesh axis runs over, the one named last changes fastest.
Arguments:
- tokens: bfloat16 [256, 4096], P(None, 'dp'), may hold values from -20 to 20
- norm_gain: float32 [2, 4096], P(None, 'dp'), may hold values from 0.1 to 1.9
- receptance: bfloat16 [2, 4096, 1024], P(None, 'dp', 'tp'), may hold values from -0.09375 to 0.09375
- key_proj: bfloat16 [2, 4096, 1024], P(None, 'dp', 'tp'), may hold values from -0.09375 to 0.09375
- value_proj: bfloat16 [2, 4096, 1024], P(None, 'dp', 'tp'), may hold values from -0.09375 to 0.09375
- decay_proj: bfloat16 [2, 4096, 1024], P(None, 'dp', 'tp'), may hold values from -0.09375 to 0.09375
- rate_proj: bfloat16 [2, 4096, 1024], P(None, 'dp', 'tp'), may hold values from -0.09375 to 0.09375
- gate_proj: bfloat16 [2, 4096, 1024], P(None, 'dp', 'tp'), may hold values from -0.09375 to 0.09375
- decay_base: float32 [2, 1024], P(None, 'tp'), may hold values from -6 to 1
- group_gain: float32 [2, 1024], P(None, 'tp'), may hold values from 0.1 to 1.9
- output_proj: bfloat16 [2, 1024, 4096], P(None, 'tp', 'dp'), may hold values from -0.1875 to 0.1875
- state: float32 [2, 256, 16, 4096], P(None, 'dp', 'tp'), may hold values from -3 to 3
Outputs:
- next_tokens: bfloat16 [256, 4096], P(None, 'dp')
- new_state: float32 [2, 256, 16, 4096], P(None, 'dp', 'tp')
All inputs are finite; a program needn't handle non-finite values.
Results may differ from a plain program's by a relative error of at most 0.0066.
Values may be sent and summed in bfloat16 or wider, within the bound.
A program may use at most 64 MiB of HBM per device.

v0:
```python
import functools

import jax
import jax.numpy as jnp
from jax import lax
from jax.experimental import pallas as pl
from jax.experimental.pallas import tpu as pltpu
from jax.sharding import PartitionSpec as P

D = 4096
HEAD = 64
LAYERS = 2


norm_floor = 0.1
group_floor = 0.5


def recurrence(state_block, recept_heads, key_heads, value_heads, decay_heads, rate_heads):
    log_rate = -jax.nn.softplus(-decay_heads) - 0.5
    forget = jnp.exp(-jnp.exp(log_rate))
    learn_rate = jax.nn.sigmoid(rate_heads)
    unit_key = key_heads * lax.rsqrt(jnp.sum(key_heads * key_heads, axis=-1, keepdims=True) + 1.0)
    scaled = key_heads * learn_rate
    removed = jnp.einsum("bhvk,bhk->bhv", state_block, -unit_key, precision=lax.Precision.HIGHEST)
    updated = (
        state_block * forget[:, :, None, :]
        + removed[..., None] * (unit_key * learn_rate)[:, :, None, :]
        + value_heads[..., None] * scaled[:, :, None, :]
    )
    read_out = jnp.einsum("bhvk,bhk->bhv", updated, recept_heads, precision=lax.Precision.HIGHEST)
    centre = read_out - jnp.mean(read_out, axis=-1, keepdims=True)
    normal = centre * lax.rsqrt(jnp.mean(centre * centre, axis=-1, keepdims=True) + group_floor)
    return (updated, normal)


def shards(
    tokens,
    norm_gain,
    receptance,
    key_proj,
    value_proj,
    decay_proj,
    rate_proj,
    gate_proj,
    decay_base,
    group_gain,
    output_proj,
    state,
):
    local_rows = state.shape[1]
    first_row = lax.axis_index("dp") * local_rows
    local_heads = state.shape[2]
    current = tokens
    finals = []
    for section_index in range(LAYERS):
        floats = current.astype(jnp.float32)
        squares = jnp.sum(floats * floats, axis=1)
        normed = (floats * norm_gain[section_index]).astype(jnp.bfloat16)
        part_recept = jnp.dot(normed, receptance[section_index], preferred_element_type=jnp.float32)
        part_key = jnp.dot(normed, key_proj[section_index], preferred_element_type=jnp.float32)
        part_value = jnp.dot(normed, value_proj[section_index], preferred_element_type=jnp.float32)
        part_decay = jnp.dot(normed, decay_proj[section_index], preferred_element_type=jnp.float32)
        part_rate = jnp.dot(normed, rate_proj[section_index], preferred_element_type=jnp.float32)
        part_gate = jnp.dot(normed, gate_proj[section_index], preferred_element_type=jnp.float32)
        totals = lax.psum(squares, "dp")
        own_squares = lax.dynamic_slice_in_dim(totals, first_row, local_rows, 0)
        summed = (
            lax.psum_scatter(part_recept, "dp", scatter_dimension=0, tiled=True),
            lax.psum_scatter(part_key, "dp", scatter_dimension=0, tiled=True),
            lax.psum_scatter(part_value, "dp", scatter_dimension=0, tiled=True),
            lax.psum_scatter(part_decay, "dp", scatter_dimension=0, tiled=True),
            lax.psum_scatter(part_rate, "dp", scatter_dimension=0, tiled=True),
            lax.psum_scatter(part_gate, "dp", scatter_dimension=0, tiled=True),
        )
        inv_rms = lax.rsqrt(own_squares / D + norm_floor)

        def by_head(term):
            rounded = lax.optimization_barrier((inv_rms[:, None] * term).astype(jnp.bfloat16))
            return rounded.astype(jnp.float32).reshape(local_rows, local_heads, HEAD)

        decay_heads = by_head(summed[3]) + decay_base[section_index].reshape(1, local_heads, HEAD)
        updated, normal = recurrence(
            state[section_index].reshape(local_rows, local_heads, HEAD, HEAD),
            by_head(summed[0]),
            by_head(summed[1]),
            by_head(summed[2]),
            decay_heads,
            by_head(summed[4]),
        )
        finals.append(updated.reshape(local_rows, local_heads, HEAD * HEAD))
        gate_value = jax.nn.sigmoid(by_head(summed[5]).reshape(local_rows, local_heads * HEAD))
        mixed_heads = (
            normal.reshape(local_rows, local_heads * HEAD) * group_gain[section_index] * gate_value
        ).astype(jnp.bfloat16)
        weights_out = output_proj[section_index]

        def apply_out(piece, begin, weights_out=weights_out):
            return jnp.dot(piece, weights_out, preferred_element_type=jnp.float32)

        partial_out = apply_out(lax.all_gather(mixed_heads, "dp", axis=0, tiled=True), jnp.int32(0))
        total = lax.psum(partial_out, "tp")
        current = (floats + total).astype(jnp.bfloat16)
    return (current, jnp.stack(finals))


MESH = pl.DeviceIdType.MESH
NT = (((1,), (1,)), ((), ()))
VMEM_LIMIT = 60 * 1024 * 1024


def remote(src, dst, send, recv, t, d):
    return pltpu.make_async_remote_copy(
        src_ref=src, dst_ref=dst, send_sem=send, recv_sem=recv, device_id={"tp": t, "dp": d}, device_id_type=MESH
    )


def greet(peers):
    barrier = pltpu.get_barrier_semaphore()
    for t, d in peers:
        pl.semaphore_signal(barrier, inc=1, device_id={"tp": t, "dp": d}, device_id_type=MESH)
    pl.semaphore_wait(barrier, len(peers))


class Lanes:
    def __init__(self, tp):
        self.t, self.d = lax.axis_index("tp"), lax.axis_index("dp")
        self.nz = tp // 4
        self.x, self.y, self.z = lax.rem(self.t, 2), lax.rem(self.t // 2, 2), self.t // 4

    def at(self, x, y, dz):
        return lax.rem(self.z + dz, self.nz) * 4 + y * 2 + x

    def peers(self):
        near = [self.at(1 - self.x, self.y, 0), self.at(self.x, 1 - self.y, 0)]
        return [(p, self.d) for p in near + [self.at(self.x, self.y, dz) for dz in range(1, self.nz)]]


def gather(lanes, buf, send, recv, beside=None, arrived=None):
    x, y, nz, d = lanes.x, lanes.y, lanes.nz, lanes.d
    xp, yp = lanes.at(1 - x, y, 0), lanes.at(x, 1 - y, 0)
    started = []
    count = [0, 0]

    def put(half, block, target):
        op = remote(buf.at[half, block], buf.at[half, block], send.at[half, count[half]], recv.at[half, block], target, d)
        count[half] += 1
        op.start()
        started.append(op)

    def got(half, block):
        remote(buf.at[half, block], buf.at[half, block], send.at[half, 0], recv.at[half, block], xp, d).wait_recv()
        if arrived is not None:
            arrived(half, block)

    zs = list(range(1, nz))
    own = lanes.t
    put(0, own, yp)
    for dz in zs:
        put(1, own, lanes.at(x, y, dz))
        put(0, own, lanes.at(x, y, dz))
    put(1, own, xp)
    put(1, own, yp)
    put(0, own, xp)
    if beside is not None:
        beside()
    got(0, yp)
    for dz in zs:
        put(0, yp, lanes.at(x, y, dz))
    put(0, yp, xp)
    got(1, xp)
    put(1, xp, yp)
    for dz in zs:
        block = lanes.at(x, y, dz)
        got(1, block)
        put(1, block, xp)
        put(1, block, yp)
        got(0, block)
        put(0, block, xp)
    for dz in zs:
        block = lanes.at(x, 1 - y, dz)
        got(0, block)
        put(0, block, xp)
        block = lanes.at(1 - x, y, dz)
        got(1, block)
        put(1, block, yp)
    for dz in range(nz):
        for k in range(2):
            got(0, lanes.at(1 - x, k, dz))
            got(1, lanes.at(k, 1 - y, dz))
    for op in started:
        op.wait_send()


def first_kernel(
    tp, tok, gain, wr, wk, wv, wd, wa, wg, wo, proj, near, w1, gain1, outw,
    tokv, w0, part, inbox, load, send, recv, a2a_send, a2a_recv, on_send, on_recv,
):
    lanes = Lanes(tp)
    t, d = lanes.t, lanes.d
    per = tp // 2
    rows, feats = tok.shape
    mine = rows // 2
    cols = feats // per
    weights = (wr, wk, wv, wd, wa, wg)
    loads = [pltpu.make_async_copy(tok, tokv, load.at[0])]
    for i, w in enumerate(weights):
        loads.append(pltpu.make_async_copy(w.at[0], w0.at[pl.ds(i * HEAD, HEAD)], load.at[1 + i]))
        loads.append(pltpu.make_async_copy(w.at[1], w1.at[d, pl.ds(i * HEAD, HEAD)], load.at[7 + i]))
    for op in loads:
        op.start()
    greet([(lax.rem(t + k, tp), d) for k in range(1, tp)] + [(t, 1 - d)])

    def spread(c):
        target = d * per + c
        return remote(wo.at[:, :, pl.ds(c * cols, cols)], outw.at[t], a2a_send.at[c], a2a_recv.at[t], target, d)

    for c in range(per):
        @pl.when(d * per + c != t)
        def _(c=c):
            spread(c).start()

        @pl.when(d * per + c == t)
        def _(c=c):
            pltpu.make_async_copy(wo.at[:, :, pl.ds(c * cols, cols)], outw.at[t], a2a_send.at[c]).start()

    loads[0].wait()
    slot = lax.rem(t, per)
    there = (1 - d) * mine
    pair = [
        remote(
            tokv.at[pl.ds(pl.multiple_of(there, mine), mine), pl.ds(pl.multiple_of(slot * cols, cols), cols)],
            near, send.at[0], recv.at[0], t, 1 - d,
        ),
        remote(gain, gain1.at[d], send.at[1], recv.at[1], t, 1 - d),
    ]
    for i, w in enumerate(weights):
        pair.append(remote(w.at[1], w1.at[d, pl.ds(i * HEAD, HEAD)], send.at[2 + i], recv.at[2 + i], t, 1 - d))
    pair[0].start()
    pair[1].start()
    gain1[pl.ds(d, 1)] = gain[...][None]

    floats = tokv[...].astype(jnp.float32)
    squares = jnp.sum(floats * floats, axis=1, keepdims=True)
    normed = (floats * gain[0:1, :]).astype(jnp.bfloat16)
    for i in range(6):
        loads[1 + 2 * i].wait()
    width = 6 * HEAD
    part[:, 0:width] = lax.dot_general(normed, w0[...], NT, preferred_element_type=jnp.float32)
    part[:, width:] = jnp.broadcast_to(squares, (rows, part.shape[1] - width))
    swap = remote(part.at[pl.ds(pl.multiple_of(there, mine), mine)], inbox, send.at[8], recv.at[8], t, 1 - d)
    swap.start()
    for op in pair[2:]:
        op.start()
    swap.wait_recv()
    total = part[pl.ds(pl.multiple_of(d * mine, mine), mine), :] + inbox[...]
    inv = lax.rsqrt(total[:, width : width + 1] / (feats * 2) + norm_floor)
    proj[...] = (inv * total[:, :width]).astype(jnp.bfloat16)

    pair[0].wait_recv()
    own = tokv[pl.ds(pl.multiple_of(d * mine, mine), mine), pl.ds(pl.multiple_of(slot * cols, cols), cols)]
    here = (t // per == d).astype(jnp.float32)
    near[...] = (own.astype(jnp.float32) * here + near[...].astype(jnp.float32) * (1.0 - here)).astype(jnp.bfloat16)

    def forward(source):
        return remote(outw.at[source], outw.at[source], on_send.at[source], on_recv.at[source], t, 1 - d)

    @pl.when(t // per == d)
    def _():
        pltpu.make_async_copy(outw.at[t], outw.at[t], a2a_send.at[slot]).wait()
        forward(t).start()
        for k in range(1, tp):
            source = lax.rem(t + k, tp)
            remote(outw.at[source], outw.at[source], a2a_send.at[0], a2a_recv.at[source], t, 1 - d).wait_recv()
            forward(source).start()

    for c in range(per):
        @pl.when(d * per + c != t)
        def _(c=c):
            spread(c).wait_send()

    @pl.when(t // per == d)
    def _():
        for k in range(tp):
            forward(k).wait_send()

    @pl.when(t // per != d)
    def _():
        for k in range(tp):
            forward(k).wait_recv()

    for op in pair[1:]:
        op.wait_recv()
    for op in pair:
        op.wait_send()
    swap.wait_send()
    for i in range(6):
        loads[2 + 2 * i].wait()


def state_kernel(proj, base, ggain, state, *rest):
    new, mixed = rest[-2], rest[-1]
    seqs = proj.shape[0]
    lines = state.shape[1] // seqs
    wide = 2 * HEAD

    def piece(i):
        return proj[:, i * HEAD : (i + 1) * HEAD].astype(jnp.float32)

    recept, key, value, decay, rate, gate = [piece(i) for i in range(6)]
    forget = jnp.exp(-jnp.exp(-jax.nn.softplus(-(decay + base[...])) - 0.5))
    scale = lax.rsqrt(jnp.sum(key * key, axis=-1, keepdims=True) + 1.0)
    learned = key * jax.nn.sigmoid(rate)

    def spread(row):
        both = jnp.concatenate([row, row], axis=-1)
        return jnp.broadcast_to(both[:, None, :], (seqs, lines, wide))

    def iota(shape, axis):
        return lax.broadcasted_iota(jnp.int32, shape, axis)

    old = state[0].reshape(seqs, lines, wide)
    lane, col = iota((wide, wide), 0), iota((wide, wide), 1)
    same = (lane // HEAD == col // HEAD).astype(jnp.bfloat16)
    odd = ((lane < HEAD) & (lane % 2 == col // HEAD)).astype(jnp.bfloat16)
    turn = (lane // HEAD == col % 2).astype(jnp.bfloat16)
    mask = (iota((lines, wide), 1) % HEAD) // 2 == iota((lines, wide), 0)

    def split(term):
        flat = term.reshape(seqs * lines, wide)
        high = flat.astype(jnp.bfloat16)
        return [high, (flat - high.astype(jnp.float32)).astype(jnp.bfloat16)]

    removed = split(old * spread(key * (-scale * scale)))
    chosen = jnp.where(mask[None], spread(value), 0.0).reshape(seqs * lines, wide).astype(jnp.bfloat16)
    rank = jnp.dot(
        jnp.concatenate(removed + [chosen], axis=1), jnp.concatenate([same, same, odd], axis=0),
        preferred_element_type=jnp.float32,
    ).reshape(seqs, lines, wide)
    updated = old * spread(forget) + rank * spread(learned)
    new[0] = updated.reshape(seqs * lines, wide)
    read = jnp.dot(
        jnp.concatenate(split(updated * spread(recept)), axis=1), jnp.concatenate([turn, turn], axis=0),
        preferred_element_type=jnp.float32,
    ).reshape(seqs, lines, wide)
    read = jnp.sum(jnp.where(mask[None], read, 0.0), axis=1)[:, :HEAD]
    centre = read - jnp.mean(read, axis=-1, keepdims=True)
    normal = centre * lax.rsqrt(jnp.mean(centre * centre, axis=-1, keepdims=True) + group_floor)
    mixed[...] = (normal * ggain[...] * jax.nn.sigmoid(gate)).astype(jnp.bfloat16)


def project_out(lanes, tp, layer, mixed, outw, near, mg, we, send, recv):
    mine, half = mixed.shape[0], mixed.shape[0] // 2
    cols = near.shape[1]
    heads = jnp.concatenate([mixed[0:half, :], mixed[half:mine, :]], axis=1)
    for k in range(2):
        mg[k, lanes.t] = heads[k * half // 2 : (k + 1) * half // 2]
    greet(lanes.peers() + [(lanes.t, 1 - lanes.d)])

    def place():
        zero = jnp.zeros((HEAD, cols), we.dtype)
        for k in range(tp):
            block = outw[k, layer]
            top, bottom = pl.ds(k * 2 * HEAD, HEAD), pl.ds(k * 2 * HEAD + HEAD, HEAD)
            we[top, 0:cols] = block
            we[top, cols : 2 * cols] = zero
            we[bottom, 0:cols] = zero
            we[bottom, cols : 2 * cols] = block

    gather(lanes, mg, send, recv, beside=place)
    packed = jnp.concatenate(
        [jnp.concatenate([mg[k, j] for j in range(tp)], axis=1) for k in range(2)], axis=0
    )
    out = jnp.dot(packed, we[...], preferred_element_type=jnp.float32)
    out = jnp.concatenate([out[:, :cols], out[:, cols:]], axis=0)
    return (near[...].astype(jnp.float32) + out).astype(jnp.bfloat16)


def middle_kernel(tp, mixed, outw, near, w1, gain1, proj, after, mg, we, xg, send, recv, xsend, xrecv, w1v, wsem):
    lanes = Lanes(tp)
    load = pltpu.make_async_copy(w1, w1v, wsem)
    load.start()
    current = project_out(lanes, tp, 0, mixed, outw, near, mg, we, send, recv)
    after[...] = current
    lane = current.shape[1] // 2
    for k in range(2):
        xg[k, lanes.t] = current[:, k * lane : (k + 1) * lane]
    gather(lanes, xg, xsend, xrecv)
    per = tp // 2
    load.wait()
    squares, part = 0.0, 0.0
    for e in range(2):
        floats = jnp.concatenate([xg[k, e * per + j] for j in range(per) for k in range(2)], axis=1).astype(jnp.float32)
        squares = squares + jnp.sum(floats * floats, axis=1, keepdims=True)
        normed = (floats * gain1[e, 1:2, :]).astype(jnp.bfloat16)
        part = part + lax.dot_general(normed, w1v[e], NT, preferred_element_type=jnp.float32)
    inv = lax.rsqrt(squares / (w1.shape[0] * w1.shape[2]) + norm_floor)
    proj[...] = (inv * part).astype(jnp.bfloat16)


def last_kernel(tp, mixed, outw, near, final, mg, we, xg, xo, send, recv, xsend, xrecv, osend, orecv):
    lanes = Lanes(tp)
    current = project_out(lanes, tp, 1, mixed, outw, near, mg, we, send, recv)
    mine, lane = current.shape[0], current.shape[1] // 2
    d, per = lanes.d, tp // 2
    for k in range(2):
        xg[k, lanes.t] = current[:, k * lane : (k + 1) * lane]

    def hand(half, block):
        place = lax.rem(block, per)
        return remote(xg.at[half, block], xo.at[half, place], osend.at[half, place], orecv.at[half, place], lanes.t, 1 - d)

    def arrived(half, block):
        @pl.when(block // per == 1 - d)
        def _():
            hand(half, block).start()

    arrived(0, lanes.t)
    arrived(1, lanes.t)
    gather(lanes, xg, xsend, xrecv, arrived=arrived)
    for j in range(per):
        for k in range(2):
            at = (2 * j + k) * lane
            final[pl.ds(pl.multiple_of(d * mine, mine), mine), at : at + lane] = xg[k, d * per + j]
    for j in range(per):
        for k in range(2):
            hand(k, (1 - d) * per + j).wait_recv()
    for j in range(per):
        for k in range(2):
            at = (2 * j + k) * lane
            final[pl.ds(pl.multiple_of((1 - d) * mine, mine), mine), at : at + lane] = xo[k, j]
    for j in range(per):
        for k in range(2):
            hand(k, (1 - d) * per + j).wait_send()


def fast(tp, tokens, norm_gain, projections, decay_base, group_gain, output_proj, state):
    rows, feats = tokens.shape
    mine, per = rows // 2, tp // 2
    cols = feats // per
    width = 6 * HEAD
    lines = HEAD * HEAD // (2 * HEAD)
    bf, f32 = jnp.bfloat16, jnp.float32
    shape = jax.ShapeDtypeStruct
    dma = pltpu.SemaphoreType.DMA
    vm, anywhere = pl.BlockSpec(memory_space=pltpu.VMEM), pl.BlockSpec(memory_space=pl.ANY)
    turned = [jnp.swapaxes(w, 1, 2) for w in projections]
    flat = state.reshape(LAYERS, mine * lines, 2 * HEAD)

    def params(number):
        return pltpu.CompilerParams(collective_id=number, has_side_effects=True, vmem_limit_bytes=VMEM_LIMIT)

    proj, near, w1, gain1, outw = pl.pallas_call(
        functools.partial(first_kernel, tp),
        out_shape=(
            shape((mine, width), bf), shape((mine, cols), bf), shape((2, width, feats), bf),
            shape((2, LAYERS, feats), f32), shape((tp, LAYERS, HEAD, cols), bf),
        ),
        in_specs=[anywhere, vm] + [anywhere] * 7,
        out_specs=(vm,) * 5,
        scratch_shapes=[
            pltpu.VMEM((rows, feats), bf), pltpu.VMEM((width, feats), bf), pltpu.VMEM((rows, width + 128), f32),
            pltpu.VMEM((mine, width + 128), f32), dma((13,)), dma((9,)), dma((9,)), dma((per,)), dma((tp,)),
            dma((tp,)), dma((tp,)),
        ],
        compiler_params=params(0),
        name="first",
    )(tokens, norm_gain, *turned, output_proj)

    seqs = min(mine, 32)

    def recur(layer, proj, filled):
        extra = [] if filled is None else [filled]
        return pl.pallas_call(
            state_kernel,
            grid=(mine // seqs,),
            out_shape=(shape(flat.shape, f32), shape((mine, HEAD), bf)),
            in_specs=[
                pl.BlockSpec((seqs, width), lambda i: (i, 0)),
                pl.BlockSpec((1, HEAD), lambda i: (0, 0)),
                pl.BlockSpec((1, HEAD), lambda i: (0, 0)),
                pl.BlockSpec((1, seqs * lines, 2 * HEAD), lambda i: (layer, i, 0)),
            ] + [anywhere] * len(extra),
            out_specs=(
                pl.BlockSpec((1, seqs * lines, 2 * HEAD), lambda i: (layer, i, 0)),
                pl.BlockSpec((seqs, HEAD), lambda i: (i, 0)),
            ),
            input_output_aliases={4: 0} if extra else {},
            compiler_params=pltpu.CompilerParams(vmem_limit_bytes=VMEM_LIMIT),
            name=f"state{layer}",
        )(proj, decay_base[layer : layer + 1], group_gain[layer : layer + 1], flat, *extra)

    filled, mixed = recur(0, proj, None)
    common = [pltpu.VMEM((2, tp, mine // 4, 2 * HEAD), bf), pltpu.VMEM((tp * 2 * HEAD, 2 * cols), bf),
              pltpu.VMEM((2, tp, mine, cols // 2), bf)]
    sems = [dma((2, tp)), dma((2, tp)), dma((2, tp)), dma((2, tp))]
    proj, near = pl.pallas_call(
        functools.partial(middle_kernel, tp),
        out_shape=(shape((mine, width), bf), shape((mine, cols), bf)),
        in_specs=[vm] * 3 + [anywhere, vm],
        out_specs=(vm,) * 2,
        scratch_shapes=common + sems + [pltpu.VMEM(w1.shape, bf), dma],
        compiler_params=params(1),
        name="middle",
    )(mixed, outw, near, w1, gain1)
    filled, mixed = recur(1, proj, filled)
    final = pl.pallas_call(
        functools.partial(last_kernel, tp),
        out_shape=shape((rows, feats), bf),
        in_specs=[vm] * 3,
        out_specs=vm,
        scratch_shapes=common + [pltpu.VMEM((2, per, mine, cols // 2), bf)] + sems + [dma((2, per)), dma((2, per))],
        compiler_params=params(2),
        name="last",
    )(mixed, outw, near)
    return (final, filled.reshape(state.shape))


def step(tp, dp, tokens, norm_gain, *rest):
    projections, (decay_base, group_gain, output_proj, state) = rest[:6], rest[6:]
    rows, feats = tokens.shape
    fits = dp == 2 and tp % 8 == 0 and state.shape[2] == 1 and state.shape[1] % 64 == 0 and (feats * dp // tp) % 256 == 0
    if fits:
        return fast(tp, tokens, norm_gain, projections, decay_base, group_gain, output_proj, state)
    return shards(tokens, norm_gain, *rest)


def solution(mesh):
    return jax.shard_map(
        functools.partial(step, mesh.shape["tp"], mesh.shape["dp"]),
        mesh=mesh,
        in_specs=(
            P(None, "dp"),
            P(None, "dp"),
            P(None, "dp", "tp"),
            P(None, "dp", "tp"),
            P(None, "dp", "tp"),
            P(None, "dp", "tp"),
            P(None, "dp", "tp"),
            P(None, "dp", "tp"),
            P(None, "tp"),
            P(None, "tp"),
            P(None, "tp", "dp"),
            P(None, "dp", "tp", None),
        ),
        out_specs=(P(None, "dp"), P(None, "dp", "tp", None)),
        check_vma=False,
    )
```

profile of v0, /device:TPU:1, one launch (start us, length us, event | category | flops | bytes accessed | tf_op | source)
XLA Modules:
  0.0 100.0 jit_solution(4460688760534653673)
XLA Ops:
  0.6 1.4 %fusion = (f32[1,64]{1,0:T(1,128)}, f32[1,64]{1,0:T(1,128)}, f32[1,64]{1,0:T(1,128)}, f32[1,64]{1,0:T(1,128)}) fusion(f32[2,64]{1,0:T(2,128)} %param.21, f32[2,64]{1,0:T(2,128)} %param.20), kind=kLoop, calls=%fused_computation | loop fusion | bytes 2048 | tf_op jit(solution)/shard_map/slice | solution.py:491
  2.0 20.1 %first.1 = (bf16[128,384]{1,0:T(8,128)(2,1)}, bf16[128,256]{1,0:T(8,128)(2,1)}, bf16[2,384,2048]{2,1,0:T(8,128)(2,1)}, f32[2,2,2048]{2,1,0:T(2,128)}, bf16[16,2,64,256]{3,2,1,0:T(8,128)(2,1)}) custom-call(bf16[256,2048]{1,0:T(8,128)(2,1)} %tok.1, f32[2,2048]{1,0:T(2,128)} %gain.1, bf16[2,64,2048]{2,1,0:T(8,128)(2,1)} %bitcast.11, ...), custom_call_target="tpu_custom_call" | custom-call | tf_op jit(solution)/shard_map/first/pallas_call | solution.py:453
  22.1 6.9 %state0.1 = (f32[2,4096,128]{2,1,0:T(8,128)}, bf16[128,64]{1,0:T(8,128)(2,1)}) custom-call(bf16[128,384]{1,0:T(8,128)(2,1)} %get-tuple-element.13.proj, f32[1,64]{1,0:T(1,128)} %get-tuple-element.30.base, f32[1,64]{1,0:T(1,128)} %get-tuple-element.27.ggain, f32[2,4096,128]{2,1,0:T(8,128)} %bitcast.8), custom_call_target="tpu_custom_call" | custom-call | tf_op jit(solution)/shard_map/state0/pallas_call | solution.py:474
  28.9 28.5 %middle.1 = (bf16[128,384]{1,0:T(8,128)(2,1)}, bf16[128,256]{1,0:T(8,128)(2,1)}) custom-call(bf16[128,64]{1,0:T(8,128)(2,1)} %get-tuple-element.14.mixed, bf16[16,2,64,256]{3,2,1,0:T(8,128)(2,1)} %get-tuple-element.15.outw, bf16[128,256]{1,0:T(8,128)(2,1)} %get-tuple-element.16.near, bf16[2,384,2048]{2,1,0:T(8,128)(2,1)} %get-tuple-element.17.w1, ...), custom_call_target="tpu_custom_call" | custom-call | tf_op jit(solution)/shard_map/middle/pallas_call | solution.py:497
  57.4 6.9 %state1.1 = (f32[2,4096,128]{2,1,0:T(8,128)}, bf16[128,64]{1,0:T(8,128)(2,1)}) custom-call(bf16[128,384]{1,0:T(8,128)(2,1)} %get-tuple-element.19.proj, f32[1,64]{1,0:T(1,128)} %get-tuple-element.31.base, f32[1,64]{1,0:T(1,128)} %get-tuple-element.26.ggain, f32[2,4096,128]{2,1,0:T(8,128)} %bitcast.9, ...), custom_call_target="tpu_custom_call", output_to_operand_aliasing={{0}: (4, {})} | custom-call | tf_op jit(solution)/shard_map/state1/pallas_call | solution.py:474
  64.3 33.4 %last.1 = bf16[256,2048]{1,0:T(8,128)(2,1)} custom-call(bf16[128,64]{1,0:T(8,128)(2,1)} %get-tuple-element.21.mixed, bf16[16,2,64,256]{3,2,1,0:T(8,128)(2,1)} %get-tuple-element.15.outw, bf16[128,256]{1,0:T(8,128)(2,1)} %get-tuple-element.22.near), custom_call_target="tpu_custom_call" | custom-call | tf_op jit(solution)/shard_map/last/pallas_call | solution.py:507
  97.7 2.3 %copy.18 = bf16[256,2048]{1,0:T(8,128)(2,1)} copy(bf16[256,2048]{1,0:T(8,128)(2,1)} %last.1) | data formatting | bytes 2097152
where the time goes:
time: 100 us
  Pallas kernels  95.7 us (96%)
  local copies, waits for them, and re-layouts  3.65 us (4%)
    pallas_call x1, Pallas kernels, fast(): pl.pallas_call(functools.partial(last_kernel, tp), out_shape=shape((rows,...  33.4 us
    pallas_call x1, Pallas kernels, fast(): pl.pallas_call(functools.partial(middle_kernel, tp), out_shape=(shape((mi...  28.5 us
    pallas_call x1, Pallas kernels, fast(): pl.pallas_call(functools.partial(first_kernel, tp), out_shape=(shape((min...  20.1 us
    pallas_call x2, Pallas kernels, recur(): pl.pallas_call(state_kernel, grid=(mine // seqs,), out_shape=(shape(flat....  13.7 us
    unnamed x1, local copies, waits for them, and re-layouts  2.3 us

commit v1 on v0

v1 whole, which is shorter than its diff:
```python
import functools

import jax
import jax.numpy as jnp
from jax import lax
from jax.experimental import pallas as pl
from jax.experimental.pallas import tpu as pltpu
from jax.sharding import PartitionSpec as P

D = 4096
HEAD = 64
LAYERS = 2


norm_floor = 0.1
group_floor = 0.5


def recurrence(state_block, recept_heads, key_heads, value_heads, decay_heads, rate_heads):
    log_rate = -jax.nn.softplus(-decay_heads) - 0.5
    forget = jnp.exp(-jnp.exp(log_rate))
    learn_rate = jax.nn.sigmoid(rate_heads)
    unit_key = key_heads * lax.rsqrt(jnp.sum(key_heads * key_heads, axis=-1, keepdims=True) + 1.0)
    scaled = key_heads * learn_rate
    removed = jnp.einsum("bhvk,bhk->bhv", state_block, -unit_key, precision=lax.Precision.HIGHEST)
    updated = (
        state_block * forget[:, :, None, :]
        + removed[..., None] * (unit_key * learn_rate)[:, :, None, :]
        + value_heads[..., None] * scaled[:, :, None, :]
    )
    read_out = jnp.einsum("bhvk,bhk->bhv", updated, recept_heads, precision=lax.Precision.HIGHEST)
    centre = read_out - jnp.mean(read_out, axis=-1, keepdims=True)
    normal = centre * lax.rsqrt(jnp.mean(centre * centre, axis=-1, keepdims=True) + group_floor)
    return (updated, normal)


def shards(
    tokens,
    norm_gain,
    receptance,
    key_proj,
    value_proj,
    decay_proj,
    rate_proj,
    gate_proj,
    decay_base,
    group_gain,
    output_proj,
    state,
):
    local_rows = state.shape[1]
    first_row = lax.axis_index("dp") * local_rows
    local_heads = state.shape[2]
    current = tokens
    finals = []
    for section_index in range(LAYERS):
        floats = current.astype(jnp.float32)
        squares = jnp.sum(floats * floats, axis=1)
        normed = (floats * norm_gain[section_index]).astype(jnp.bfloat16)
        part_recept = jnp.dot(normed, receptance[section_index], preferred_element_type=jnp.float32)
        part_key = jnp.dot(normed, key_proj[section_index], preferred_element_type=jnp.float32)
        part_value = jnp.dot(normed, value_proj[section_index], preferred_element_type=jnp.float32)
        part_decay = jnp.dot(normed, decay_proj[section_index], preferred_element_type=jnp.float32)
        part_rate = jnp.dot(normed, rate_proj[section_index], preferred_element_type=jnp.float32)
        part_gate = jnp.dot(normed, gate_proj[section_index], preferred_element_type=jnp.float32)
        totals = lax.psum(squares, "dp")
        own_squares = lax.dynamic_slice_in_dim(totals, first_row, local_rows, 0)
        summed = (
            lax.psum_scatter(part_recept, "dp", scatter_dimension=0, tiled=True),
            lax.psum_scatter(part_key, "dp", scatter_dimension=0, tiled=True),
            lax.psum_scatter(part_value, "dp", scatter_dimension=0, tiled=True),
            lax.psum_scatter(part_decay, "dp", scatter_dimension=0, tiled=True),
            lax.psum_scatter(part_rate, "dp", scatter_dimension=0, tiled=True),
            lax.psum_scatter(part_gate, "dp", scatter_dimension=0, tiled=True),
        )
        inv_rms = lax.rsqrt(own_squares / D + norm_floor)

        def by_head(term):
            rounded = lax.optimization_barrier((inv_rms[:, None] * term).astype(jnp.bfloat16))
            return rounded.astype(jnp.float32).reshape(local_rows, local_heads, HEAD)

        decay_heads = by_head(summed[3]) + decay_base[section_index].reshape(1, local_heads, HEAD)
        updated, normal = recurrence(
            state[section_index].reshape(local_rows, local_heads, HEAD, HEAD),
            by_head(summed[0]),
            by_head(summed[1]),
            by_head(summed[2]),
            decay_heads,
            by_head(summed[4]),
        )
        finals.append(updated.reshape(local_rows, local_heads, HEAD * HEAD))
        gate_value = jax.nn.sigmoid(by_head(summed[5]).reshape(local_rows, local_heads * HEAD))
        mixed_heads = (
            normal.reshape(local_rows, local_heads * HEAD) * group_gain[section_index] * gate_value
        ).astype(jnp.bfloat16)
        weights_out = output_proj[section_index]

        def apply_out(piece, begin, weights_out=weights_out):
            return jnp.dot(piece, weights_out, preferred_element_type=jnp.float32)

        partial_out = apply_out(lax.all_gather(mixed_heads, "dp", axis=0, tiled=True), jnp.int32(0))
        total = lax.psum(partial_out, "tp")
        current = (floats + total).astype(jnp.bfloat16)
    return (current, jnp.stack(finals))


MESH = pl.DeviceIdType.MESH
NT = (((1,), (1,)), ((), ()))
PAIR = 2 * HEAD
VMEM_LIMIT = 57 * 1024 * 1024


class Grid:
    def __init__(self, tp):
        self.tp, self.nz, self.per = tp, tp // 4, tp // 2
        self.t, self.d = lax.axis_index("tp"), lax.axis_index("dp")
        self.z = self.t // 4
        x, y = lax.rem(self.t, 2), lax.rem(self.t // 2, 2)
        self.xp, self.yp = self.t + 1 - 2 * x, self.t + 2 - 4 * y
        self.xyp = self.xp + self.yp - self.t
        order = [sorted((k for k in range(self.nz) if k != z), key=lambda k: abs(k - z)) for z in range(self.nz)]
        self.line = []
        for k in range(self.nz - 1):
            level = order[0][k]
            for z in range(1, self.nz):
                level = jnp.where(self.z == z, order[z][k], level)
            self.line.append(level * 4 + lax.rem(self.t, 4))

    def over(self, base, chip):
        return base // 4 * 4 + lax.rem(chip, 4)

    def lots(self):
        return [self.t] + self.line


class Sender:
    def __init__(self, sems):
        self.sems, self.ops = sems, []

    def put(self, src, dst, recv, t, d, when=None):
        op = pltpu.make_async_remote_copy(
            src_ref=src, dst_ref=dst, send_sem=self.sems.at[len(self.ops)], recv_sem=recv,
            device_id={"tp": t, "dp": d}, device_id_type=MESH,
        )
        self.ops.append((op, when))
        if when is None:
            op.start()
        else:
            pl.when(when)(op.start)

    def drain(self):
        for op, when in self.ops:
            if when is None:
                op.wait_send()
            else:
                pl.when(when)(op.wait_send)
        self.ops = []


def landed(ref, recv, grid):
    pltpu.make_async_remote_copy(
        src_ref=ref, dst_ref=ref, send_sem=recv, recv_sem=recv,
        device_id={"tp": grid.xp, "dp": grid.d}, device_id_type=MESH,
    ).wait_recv()


def gather_heads(grid, buf, out, recv, beside):
    def put(block, chip):
        out.put(buf.at[block], buf.at[block], recv.at[block], chip, grid.d)

    for chip in grid.line[::-1] + [grid.xyp, grid.xp, grid.yp]:
        put(grid.t, chip)
    beside()
    for block in grid.line:
        landed(buf.at[block], recv.at[block], grid)
        for chip in (grid.xyp, grid.xp, grid.yp):
            put(block, chip)
    for lot in grid.lots():
        for chip in (grid.xp, grid.yp, grid.xyp):
            block = grid.over(lot, chip)
            landed(buf.at[block], recv.at[block], grid)


def gather_tiles(grid, buf, out, recv, use):
    def put(block, half, chip):
        out.put(buf.at[block, half], buf.at[block, half], recv.at[block, half], chip, grid.d)

    def got(block, half):
        landed(buf.at[block, half], recv.at[block, half], grid)

    def plane(block):
        put(block, 0, grid.xp)
        put(block, 1, grid.yp)
        put(block, 1, grid.xp)
        put(block, 0, grid.yp)

    def relay(lot):
        across, along = grid.over(lot, grid.xp), grid.over(lot, grid.yp)
        got(across, 0)
        put(across, 0, grid.yp)
        got(along, 1)
        put(along, 1, grid.xp)

    for half in range(2):
        for chip in grid.line:
            put(grid.t, half, chip)
    plane(grid.t)
    last = grid.t
    for block in grid.line:
        got(block, 0)
        got(block, 1)
        plane(block)
        relay(last)
        last = block
    relay(last)
    for lot in grid.lots():
        across, along, corner = grid.over(lot, grid.xp), grid.over(lot, grid.yp), grid.over(lot, grid.xyp)
        got(across, 1)
        got(along, 0)
        got(corner, 0)
        got(corner, 1)
        for block in (lot, across, along, corner):
            use(block)


def spread_result(grid, tile, final, out, recv):
    rows, lane = tile.shape[1], tile.shape[2]
    d, per, half_z = grid.d, grid.per, grid.nz // 2
    home = grid.t // per

    def place(block, r, half):
        at = pl.multiple_of((lax.rem(block, per) * 2 + half) * lane, lane)
        return final.at[pl.ds(pl.multiple_of(r * rows, rows), rows), pl.ds(at, lane)]

    def sem(block, r, half):
        return recv.at[lax.rem(block, per), r, half]

    def own(half, chip, when=None):
        out.put(tile.at[half], place(grid.t, d, half), sem(grid.t, d, half), chip, home, when)

    def put(block, r, half, chip, when=None):
        out.put(place(block, r, half), place(block, r, half), sem(block, r, half), chip, d, when)

    def got(block, r, half, when=None):
        def wait():
            landed(place(block, r, half), sem(block, r, half), grid)

        if when is None:
            wait()
        else:
            pl.when(when)(wait)

    away = home != d
    for half in range(2):
        for chip in grid.line:
            own(half, chip)
    own(0, grid.xp)
    own(1, grid.yp)
    own(1, grid.xp)
    own(0, grid.yp)
    for half in range(2):
        own(half, grid.t, away)

        @pl.when(home == d)
        def _(half=half):
            place(grid.t, d, half)[...] = tile[half]

    low = d * half_z
    lots = []
    for k in range(half_z):
        inside = low + lax.rem(grid.z - low + half_z + k, half_z)
        level = jnp.where(grid.z < low, low + k, jnp.where(grid.z >= low + half_z, low + half_z - 1 - k, inside))
        lots.append((level * 4 + lax.rem(grid.t, 4), level != grid.z))

    def relay(lot):
        across, along = grid.over(lot, grid.xp), grid.over(lot, grid.yp)
        for r in range(2):
            got(across, r, 0)
            put(across, r, 0, grid.yp)
            got(along, r, 1)
            put(along, r, 1, grid.xp)

    for lot, far in lots:
        for r in range(2):
            for half in range(2):
                got(lot, r, half, far)
            put(lot, r, 0, grid.xp, far)
            put(lot, r, 1, grid.yp, far)
            put(lot, r, 1, grid.xp, far)
            put(lot, r, 0, grid.yp, far)
        relay(lot)
    for lot, far in lots:
        across, along, corner = grid.over(lot, grid.xp), grid.over(lot, grid.yp), grid.over(lot, grid.xyp)
        for r in range(2):
            for half in range(2):
                got(lot, r, half, jnp.logical_and(jnp.logical_not(far), r != d))
            got(across, r, 1)
            got(along, r, 0)
            got(corner, r, 0)
            got(corner, r, 1)


def iota(shape, axis):
    return lax.broadcasted_iota(jnp.int32, shape, axis)


def update_state(proj, base, ggain, layer, old, new, terms, reads, seqs):
    mine = proj.shape[0]
    lines = old.shape[1] // mine

    def piece(i):
        return proj[:, i * HEAD : (i + 1) * HEAD].astype(jnp.float32)

    recept, key, value, decay, rate = [piece(i) for i in range(5)]
    scale = lax.rsqrt(jnp.sum(key * key, axis=-1, keepdims=True) + 1.0)
    forget = jnp.exp(-jnp.exp(-jax.nn.softplus(-(decay + base[layer : layer + 1, :])) - 0.5))
    learned = key * jax.nn.sigmoid(rate)
    for i, term in enumerate((key * (-scale * scale), forget, learned, recept, value)):
        terms[i] = jnp.concatenate([term, term], axis=-1)

    lane, col = iota((PAIR, PAIR), 0), iota((PAIR, PAIR), 1)
    same = (lane // HEAD == col // HEAD).astype(jnp.bfloat16)
    odd = ((lane < HEAD) & (lane % 2 == col // HEAD)).astype(jnp.bfloat16)
    turn = (lane // HEAD == col % 2).astype(jnp.bfloat16)
    both = jnp.concatenate([same, odd], axis=0)
    mask = (iota((lines, PAIR), 1) % HEAD) // 2 == iota((lines, PAIR), 0)

    def step(i, carry):
        begin = pl.multiple_of(i * seqs, seqs)
        first = pl.multiple_of(i * seqs * lines, seqs * lines)

        def spread(k):
            return jnp.broadcast_to(terms[k, pl.ds(begin, seqs), :][:, None, :], (seqs, lines, PAIR))

        state = old[layer, pl.ds(first, seqs * lines), :].reshape(seqs, lines, PAIR)
        product = (state * spread(0)).astype(jnp.bfloat16).reshape(seqs * lines, PAIR)
        chosen = jnp.where(mask[None], spread(4), 0.0).astype(jnp.bfloat16).reshape(seqs * lines, PAIR)
        rank = jnp.dot(jnp.concatenate([product, chosen], axis=1), both, preferred_element_type=jnp.float32)
        updated = state * spread(1) + rank.reshape(seqs, lines, PAIR) * spread(2)
        new[layer, pl.ds(first, seqs * lines), :] = updated.reshape(seqs * lines, PAIR)
        weighed = (updated * spread(3)).astype(jnp.bfloat16).reshape(seqs * lines, PAIR)
        read = jnp.dot(weighed, turn, preferred_element_type=jnp.float32).reshape(seqs, lines, PAIR)
        reads[pl.ds(begin, seqs), :] = jnp.sum(jnp.where(mask[None], read, 0.0), axis=1)
        return carry

    lax.fori_loop(0, mine // seqs, step, 0)
    read = reads[:, :HEAD]
    centre = read - jnp.mean(read, axis=-1, keepdims=True)
    normal = centre * lax.rsqrt(jnp.mean(centre * centre, axis=-1, keepdims=True) + group_floor)
    return (normal * ggain[layer : layer + 1, :] * jax.nn.sigmoid(piece(5))).astype(jnp.bfloat16)


def whole_kernel(
    tp, tok, gain, wr, wk, wv, wd, wa, wg, wo, base_in, ggain_in, state, final, new,
    tokv, w0, w1, gains, part, inbox, acc, near, outw, we, mg, xg, tile, old, terms, reads, proj, base, ggain,
    load, pair_send, pair_recv, a2a_send, a2a_recv, on_send, on_recv, m_send, m_recv, x_send, x_recv, f_send, f_recv,
):
    grid = Grid(tp)
    t, d, per = grid.t, grid.d, grid.per
    rows, feats = tok.shape
    mine = rows // 2
    cols = near.shape[1]
    width = 6 * HEAD
    weights = (wr, wk, wv, wd, wa, wg)
    here, there = pl.multiple_of(d * mine, mine), pl.multiple_of((1 - d) * mine, mine)

    def copy(src, dst, number):
        return pltpu.make_async_copy(src, dst, load.at[number])

    get_there = copy(tok.at[pl.ds(there, mine)], tokv.at[pl.ds(there, mine)], 0)
    get_here = copy(tok.at[pl.ds(here, mine)], tokv.at[pl.ds(here, mine)], 1)
    get_gain = copy(gain, gains.at[d], 2)
    get_base, get_ggain = copy(base_in, base, 3), copy(ggain_in, ggain, 4)
    get_w0 = [copy(w.at[0], w0.at[pl.ds(i * HEAD, HEAD)], 5 + i) for i, w in enumerate(weights)]
    get_w1 = [copy(w.at[1], w1.at[d, pl.ds(i * HEAD, HEAD)], 11 + i) for i, w in enumerate(weights)]
    get_state = [copy(state.at[k], old.at[k], 17 + k) for k in range(LAYERS)]
    for op in [get_there, get_gain] + get_w0 + [get_here, get_base, get_ggain]:
        op.start()

    barrier = pltpu.get_barrier_semaphore()
    for k in range(1, tp):
        for core in range(2):
            pl.semaphore_signal(barrier, inc=1, device_id={"tp": lax.rem(t + k, tp), "dp": core}, device_id_type=MESH)
    pl.semaphore_signal(barrier, inc=1, device_id={"tp": t, "dp": 1 - d}, device_id_type=MESH)
    for op in [get_state[0]] + get_w1 + [get_state[1]]:
        op.start()

    def project(begin):
        floats = tokv[pl.ds(begin, mine), :].astype(jnp.float32)
        part[pl.ds(begin, mine), width:] = jnp.broadcast_to(jnp.sum(floats * floats, axis=1, keepdims=True), (mine, PAIR))
        normed = (floats * gains[d, 0:1, :]).astype(jnp.bfloat16)
        part[pl.ds(begin, mine), 0:width] = lax.dot_general(normed, w0[...], NT, preferred_element_type=jnp.float32)

    for op in [get_there, get_gain] + get_w0:
        op.wait()
    project(there)
    pl.semaphore_wait(barrier, 2 * tp - 1)

    pair = Sender(pair_send)
    pair.put(part.at[pl.ds(there, mine)], inbox, pair_recv.at[0], t, 1 - d)
    slot = lax.rem(t, per)
    slot_cols = pl.ds(pl.multiple_of(slot * cols, cols), cols)
    pair.put(tokv.at[pl.ds(there, mine), slot_cols], near, pair_recv.at[1], t, 1 - d)
    pair.put(gains.at[d], gains.at[d], pair_recv.at[2], t, 1 - d)

    a2a = [Sender(a2a_send.at[k]) for k in range(LAYERS)]
    home = t // per == d

    def spread_weights(layer):
        for c in range(per):
            block = wo.at[layer, :, pl.ds(c * cols, cols)]
            target = d * per + c
            a2a[layer].put(block, outw.at[layer, t], a2a_recv.at[layer, t], target, d, when=target != t)

            @pl.when(target == t)
            def _(block=block):
                pltpu.make_async_copy(block, outw.at[layer, t], a2a_recv.at[layer, t]).start()

    spread_weights(0)
    for i, w in enumerate(weights):
        block = w1.at[d, pl.ds(i * HEAD, HEAD)]
        pair.put(w.at[1], block, pair_recv.at[3 + i], t, 1 - d)
    spread_weights(1)

    get_here.wait()
    project(here)
    get_base.wait()
    get_ggain.wait()
    landed(inbox, pair_recv.at[0], grid)
    total = part[pl.ds(here, mine), :] + inbox[...]
    inv = lax.rsqrt(total[:, width : width + 1] / (feats * 2) + norm_floor)
    proj[...] = (inv * total[:, :width]).astype(jnp.bfloat16)

    landed(near, pair_recv.at[1], grid)
    own = tokv[pl.ds(here, mine), slot_cols].astype(jnp.float32)
    ours = home.astype(jnp.float32)
    current = own * ours + near[...].astype(jnp.float32) * (1.0 - ours)

    forwards = [Sender(on_send.at[k]) for k in range(LAYERS)]

    def forward_weights(layer):
        for k in range(tp):
            source = lax.rem(t + k, tp)
            block, arrived, onward = outw.at[layer, source], a2a_recv.at[layer, source], on_recv.at[layer, source]
            if k == 0:
                @pl.when(home)
                def _(block=block, arrived=arrived):
                    pltpu.make_async_copy(block, block, arrived).wait()
            else:
                @pl.when(home)
                def _(block=block, arrived=arrived):
                    landed(block, arrived, grid)
            forwards[layer].put(block, block, onward, t, 1 - d, when=home)
        for k in range(tp):
            @pl.when(jnp.logical_not(home))
            def _(k=k):
                landed(outw.at[layer, k], on_recv.at[layer, k], grid)

    def project_out(layer, mixed, current):
        half = mine // 2
        mg[layer, t] = jnp.concatenate([mixed[0:half, :], mixed[half:mine, :]], axis=1)
        heads = Sender(m_send.at[layer])

        def beside():
            forward_weights(layer)
            zero = jnp.zeros((HEAD, cols), we.dtype)
            for k in range(tp):
                block = outw[layer, k]
                top, bottom = pl.ds(k * PAIR, HEAD), pl.ds(k * PAIR + HEAD, HEAD)
                we[top, 0:cols] = block
                we[top, cols : 2 * cols] = zero
                we[bottom, 0:cols] = zero
                we[bottom, cols : 2 * cols] = block

        gather_heads(grid, mg.at[layer], heads, m_recv.at[layer], beside)
        packed = jnp.concatenate([mg[layer, j] for j in range(tp)], axis=1)
        out = jnp.dot(packed, we[...], preferred_element_type=jnp.float32)
        out = jnp.concatenate([out[:, :cols], out[:, cols:]], axis=0)
        heads.drain()
        return (current + out).astype(jnp.bfloat16)

    seqs = min(mine, 16)
    get_state[0].wait()
    mixed = update_state(proj, base, ggain, 0, old, new, terms, reads, seqs)
    stream = project_out(0, mixed, current)

    lane = cols // 2
    for k in range(2):
        xg[t, k] = stream[:, k * lane : (k + 1) * lane]
    for op in get_w1:
        op.wait()
    for i in range(6):
        landed(w1.at[1 - d, pl.ds(i * HEAD, HEAD)], pair_recv.at[3 + i], grid)
    landed(gains.at[1 - d], pair_recv.at[2], grid)
    acc[...] = jnp.zeros(acc.shape, jnp.float32)

    def use(block):
        half, at = block // per, pl.multiple_of(lax.rem(block, per) * cols, cols)
        floats = jnp.concatenate([xg[block, k] for k in range(2)], axis=1).astype(jnp.float32)
        normed = (floats * gains[half, 1:2, pl.ds(at, cols)]).astype(jnp.bfloat16)
        weight = w1[half, :, pl.ds(at, cols)]
        acc[:, 0:width] += lax.dot_general(normed, weight, NT, preferred_element_type=jnp.float32)
        squares = floats * floats
        for k in range(cols // PAIR):
            acc[:, width:] += squares[:, k * PAIR : (k + 1) * PAIR]

    tiles = Sender(x_send)
    gather_tiles(grid, xg, tiles, x_recv, use)
    inv = lax.rsqrt(jnp.sum(acc[:, width:], axis=1, keepdims=True) / (feats * 2) + norm_floor)
    proj[...] = (inv * acc[:, 0:width]).astype(jnp.bfloat16)

    get_state[1].wait()
    mixed = update_state(proj, base, ggain, 1, old, new, terms, reads, seqs)
    stream = project_out(1, mixed, stream.astype(jnp.float32))
    for k in range(2):
        tile[k] = stream[:, k * lane : (k + 1) * lane]
    finish = Sender(f_send)
    spread_result(grid, tile, final, finish, f_recv)

    for sender in [pair, tiles, finish] + a2a + forwards:
        sender.drain()


def store_kernel(final, new, final_out, new_out, sems):
    ops = [pltpu.make_async_copy(new, new_out, sems.at[0]), pltpu.make_async_copy(final, final_out, sems.at[1])]
    for op in ops:
        op.start()
    for op in ops:
        op.wait()


def fast(tp, tokens, norm_gain, projections, decay_base, group_gain, output_proj, state):
    rows, feats = tokens.shape
    mine, per = rows // 2, tp // 2
    cols = feats // per
    width = 6 * HEAD
    lines = HEAD * HEAD // PAIR
    bf, f32 = jnp.bfloat16, jnp.float32
    shape, vmem, dma = jax.ShapeDtypeStruct, pltpu.VMEM, pltpu.SemaphoreType.DMA
    inside, anywhere = pl.BlockSpec(memory_space=pltpu.VMEM), pl.BlockSpec(memory_space=pl.ANY)
    turned = [jnp.swapaxes(w, 1, 2) for w in projections]
    flat = state.reshape(LAYERS, mine * lines, PAIR)
    outs = (shape((rows, feats), bf), shape(flat.shape, f32))
    final, new = pl.pallas_call(
        functools.partial(whole_kernel, tp),
        out_shape=(vmem((rows, feats), bf), vmem(flat.shape, f32)),
        in_specs=[pl.BlockSpec(memory_space=pltpu.HBM)] * 12,
        out_specs=(inside, inside),
        scratch_shapes=[
            vmem((rows, feats), bf), vmem((width, feats), bf), vmem((2, width, feats), bf), vmem((2, LAYERS, feats), f32),
            vmem((rows, width + PAIR), f32), vmem((mine, width + PAIR), f32), vmem((mine, width + PAIR), f32),
            vmem((mine, cols), bf),
            vmem((LAYERS, tp, HEAD, cols), bf), vmem((tp * PAIR, 2 * cols), bf), vmem((LAYERS, tp, mine // 2, PAIR), bf),
            vmem((tp, 2, mine, cols // 2), bf), vmem((2, mine, cols // 2), bf), vmem(flat.shape, f32),
            vmem((5, mine, PAIR), f32), vmem((mine, PAIR), f32), vmem((mine, width), bf),
            vmem((LAYERS, HEAD), f32), vmem((LAYERS, HEAD), f32),
            dma((19,)), dma((9,)), dma((9,)), dma((LAYERS, per)), dma((LAYERS, tp)), dma((LAYERS, tp)), dma((LAYERS, tp)),
            dma((LAYERS, 4 * tp)), dma((LAYERS, tp)), dma((8 * tp,)), dma((tp, 2)), dma((8 * tp,)), dma((per, 2, 2)),
        ],
        compiler_params=pltpu.CompilerParams(collective_id=0, has_side_effects=True, vmem_limit_bytes=VMEM_LIMIT),
        name="whole",
    )(tokens, norm_gain, *turned, output_proj, decay_base, group_gain, flat)
    final, new = pl.pallas_call(
        store_kernel,
        out_shape=outs,
        in_specs=[inside, inside],
        out_specs=(anywhere, anywhere),
        scratch_shapes=[dma((2,))],
        compiler_params=pltpu.CompilerParams(vmem_limit_bytes=1024 * 1024),
        name="store",
    )(final, new)
    return (final, new.reshape(state.shape))


def step(tp, dp, tokens, norm_gain, *rest):
    projections, (decay_base, group_gain, output_proj, state) = rest[:6], rest[6:]
    rows, feats = tokens.shape
    fits = dp == 2 and tp % 8 == 0 and state.shape[2] == 1 and state.shape[1] % 64 == 0 and (feats * dp // tp) % 256 == 0
    if fits:
        return fast(tp, tokens, norm_gain, projections, decay_base, group_gain, output_proj, state)
    return shards(tokens, norm_gain, *rest)


def solution(mesh):
    return jax.shard_map(
        functools.partial(step, mesh.shape["tp"], mesh.shape["dp"]),
        mesh=mesh,
        in_specs=(
            P(None, "dp"),
            P(None, "dp"),
            P(None, "dp", "tp"),
            P(None, "dp", "tp"),
            P(None, "dp", "tp"),
            P(None, "dp", "tp"),
            P(None, "dp", "tp"),
            P(None, "dp", "tp"),
            P(None, "tp"),
            P(None, "tp"),
            P(None, "tp", "dp"),
            P(None, "dp", "tp", None),
        ),
        out_specs=(P(None, "dp"), P(None, "dp", "tp", None)),
        check_vma=False,
    )
```

time: 100 us -> 74.5 us (0.74)
  Pallas kernels: 95.7 us -> 73.7 us
  local copies, waits for them, and re-layouts: 3.65 us -> 0 us
    pallas_call x5 -> x2, Pallas kernels: 95.7 us -> 73.7 us  [the longest x1 71.3 us: fast(): pl.pallas_call(functools.partial(whole_kernel, tp), out_shape=(vmem((rows...]
    unnamed x1 -> x0, local copies, waits for them, and re-layouts: 2.3 us -> none
    slice x1 -> x0, local copies, waits for them, and re-layouts: 1.35 us -> none  [recur(): group_gain[layer:layer + 1]]
where the time goes in v1:
time: 74.5 us; the launch traced here: 74.3 us
  Pallas kernels  73.7 us (99%)
    pallas_call x1, Pallas kernels, fast(): pl.pallas_call(functools.partial(whole_kernel, tp), out_shape=(vmem((rows...  71.3 us
    pallas_call x1, Pallas kernels, fast(): pl.pallas_call(store_kernel, out_shape=outs, in_specs=[inside, inside], o...  2.37 us

profile of v1, /device:TPU:1, one launch (start us, length us, event | category | flops | bytes accessed | tf_op | source)
XLA Modules:
  0.0 74.3 jit_solution(6019658872526085995)
XLA Ops:
  0.6 71.3 %whole.1 = (bf16[256,2048]{1,0:T(8,128)(2,1)S(1)}, f32[2,4096,128]{2,1,0:T(8,128)S(1)}) custom-call(bf16[256,2048]{1,0:T(8,128)(2,1)} %tok.1, f32[2,2048]{1,0:T(2,128)} %gain.1, bf16[2,64,2048]{2,1,0:T(8,128)(2,1)} %bitcast.9, bf16[2,64,2048]{2,1,0:T(8,128)(2,1)} %bitcast.10, bf16[2,64,2048]{2,1,0:T(8,128)(2,1)} %bitcast.11, bf16[2,64,2048]{2,1,0:T(8,128)(2,1)} %bitcast.12, ...), custom_call_target="tpu_custom_call" | custom-call | tf_op jit(solution)/shard_map/whole/pallas_call | solution.py:544
  71.9 2.4 %store.1 = (bf16[256,2048]{1,0:T(8,128)(2,1)}, f32[2,4096,128]{2,1,0:T(8,128)}) custom-call(bf16[256,2048]{1,0:T(8,128)(2,1)S(1)} %get-tuple-element.6.final, f32[2,4096,128]{2,1,0:T(8,128)S(1)} %get-tuple-element.7.new), custom_call_target="tpu_custom_call" | custom-call | tf_op jit(solution)/shard_map/store/pallas_call | solution.py:563

commit v2 on v1

--- a/solution.py
+++ b/solution.py
@@ -134,132 +134,131 @@
 
 
 class Sender:
-    def __init__(self, sems):
-        self.sems, self.ops = sems, []
+    def __init__(self, sem):
+        self.sem = sem
 
     def put(self, src, dst, recv, t, d, when=None):
         op = pltpu.make_async_remote_copy(
-            src_ref=src, dst_ref=dst, send_sem=self.sems.at[len(self.ops)], recv_sem=recv,
+            src_ref=src, dst_ref=dst, send_sem=self.sem, recv_sem=recv,
             device_id={"tp": t, "dp": d}, device_id_type=MESH,
         )
-        self.ops.append((op, when))
         if when is None:
             op.start()
         else:
             pl.when(when)(op.start)
 
-    def drain(self):
-        for op, when in self.ops:
-            if when is None:
-                op.wait_send()
-            else:
-                pl.when(when)(op.wait_send)
-        self.ops = []
-
-
-def landed(ref, recv, grid):
-    pltpu.make_async_remote_copy(
-        src_ref=ref, dst_ref=ref, send_sem=recv, recv_sem=recv,
+
+def whole_of(ref, sem, grid):
+    return pltpu.make_async_remote_copy(
+        src_ref=ref, dst_ref=ref, send_sem=sem, recv_sem=sem,
         device_id={"tp": grid.xp, "dp": grid.d}, device_id_type=MESH,
-    ).wait_recv()
-
-
-def gather_heads(grid, buf, out, recv, beside):
-    def put(block, chip):
-        out.put(buf.at[block], buf.at[block], recv.at[block], chip, grid.d)
-
-    for chip in grid.line[::-1] + [grid.xyp, grid.xp, grid.yp]:
-        put(grid.t, chip)
+    )
+
+
+def landed(ref, recv, grid, when=None):
+    op = whole_of(ref, recv, grid)
+    if when is None:
+        op.wait_recv()
+    else:
+        pl.when(when)(op.wait_recv)
+
+
+def left(ref, send, grid, when=None):
+    op = whole_of(ref, send, grid)
+    if when is None:
+        op.wait_send()
+    else:
+        pl.when(when)(op.wait_send)
+
+
+def gather_heads(grid, buf, send, line, plane, beside):
+    out = Sender(send)
+    for chip in grid.line[::-1]:
+        out.put(buf.at[grid.t], buf.at[grid.t], line.at[grid.z], chip, grid.d)
+    for chip in (grid.xyp, grid.xp, grid.yp):
+        out.put(buf.at[grid.t], buf.at[grid.t], plane, chip, grid.d)
     beside()
     for block in grid.line:
-        landed(buf.at[block], recv.at[block], grid)
+        landed(buf.at[block], line.at[block // 4], grid)
         for chip in (grid.xyp, grid.xp, grid.yp):
-            put(block, chip)
-    for lot in grid.lots():
-        for chip in (grid.xp, grid.yp, grid.xyp):
-            block = grid.over(lot, chip)
-            landed(buf.at[block], recv.at[block], grid)
-
-
-def gather_tiles(grid, buf, out, recv, use):
-    def put(block, half, chip):
-        out.put(buf.at[block, half], buf.at[block, half], recv.at[block, half], chip, grid.d)
-
-    def got(block, half):
-        landed(buf.at[block, half], recv.at[block, half], grid)
+            out.put(buf.at[block], buf.at[block], plane, chip, grid.d)
+    landed(buf.at[0 : 3 * grid.nz], plane, grid)
+    left(buf.at[0 : 4 * grid.nz - 1], send, grid)
+
+
+def gather_tiles(grid, buf, send, line, relayed, rest, after, use):
+    out = Sender(send)
+
+    def put(block, half, recv, chip):
+        out.put(buf.at[block, half], buf.at[block, half], recv, chip, grid.d)
 
     def plane(block):
-        put(block, 0, grid.xp)
-        put(block, 1, grid.yp)
-        put(block, 1, grid.xp)
-        put(block, 0, grid.yp)
+        level = block // 4
+        put(block, 0, relayed.at[level, 0], grid.xp)
+        put(block, 1, relayed.at[level, 1], grid.yp)
+        put(block, 1, rest.at[level], grid.xp)
+        put(block, 0, rest.at[level], grid.yp)
 
     def relay(lot):
-        across, along = grid.over(lot, grid.xp), grid.over(lot, grid.yp)
-        got(across, 0)
-        put(across, 0, grid.yp)
-        got(along, 1)
-        put(along, 1, grid.xp)
+        across, along, level = grid.over(lot, grid.xp), grid.over(lot, grid.yp), lot // 4
+        landed(buf.at[across, 0], relayed.at[level, 0], grid)
+        put(across, 0, rest.at[level], grid.yp)
+        landed(buf.at[along, 1], relayed.at[level, 1], grid)
+        put(along, 1, rest.at[level], grid.xp)
 
     for half in range(2):
         for chip in grid.line:
-            put(grid.t, half, chip)
+            put(grid.t, half, line.at[grid.z], chip)
     plane(grid.t)
     last = grid.t
     for block in grid.line:
-        got(block, 0)
-        got(block, 1)
+        landed(buf.at[block], line.at[block // 4], grid)
         plane(block)
         relay(last)
         last = block
     relay(last)
+    after()
     for lot in grid.lots():
-        across, along, corner = grid.over(lot, grid.xp), grid.over(lot, grid.yp), grid.over(lot, grid.xyp)
-        got(across, 1)
-        got(along, 0)
-        got(corner, 0)
-        got(corner, 1)
-        for block in (lot, across, along, corner):
+        landed(buf.at[0:2], rest.at[lot // 4], grid)
+        for block in (lot, grid.over(lot, grid.xp), grid.over(lot, grid.yp), grid.over(lot, grid.xyp)):
             use(block)
 
-
-def spread_result(grid, tile, final, out, recv):
+    def finish():
+        left(buf.at[0 : 4 * grid.nz - 1], send, grid)
+
+    return finish
+
+
+def spread_result(grid, tile, final, send, line, relayed, rest):
     rows, lane = tile.shape[1], tile.shape[2]
     d, per, half_z = grid.d, grid.per, grid.nz // 2
     home = grid.t // per
+    out, extra = Sender(send.at[0]), Sender(send.at[1])
 
     def place(block, r, half):
         at = pl.multiple_of((lax.rem(block, per) * 2 + half) * lane, lane)
         return final.at[pl.ds(pl.multiple_of(r * rows, rows), rows), pl.ds(at, lane)]
 
-    def sem(block, r, half):
-        return recv.at[lax.rem(block, per), r, half]
-
-    def own(half, chip, when=None):
-        out.put(tile.at[half], place(grid.t, d, half), sem(grid.t, d, half), chip, home, when)
-
-    def put(block, r, half, chip, when=None):
-        out.put(place(block, r, half), place(block, r, half), sem(block, r, half), chip, d, when)
-
-    def got(block, r, half, when=None):
-        def wait():
-            landed(place(block, r, half), sem(block, r, half), grid)
-
-        if when is None:
-            wait()
-        else:
-            pl.when(when)(wait)
+    def share(count):
+        return final.at[pl.ds(0, count * rows // (2 * per))]
+
+    def deep(block):
+        return lax.rem(block // 4, half_z)
+
+    def own(half, recv, chip, when=None):
+        (out if when is None else extra).put(tile.at[half], place(grid.t, d, half), recv, chip, home, when)
 
     away = home != d
+    level = deep(grid.t)
     for half in range(2):
         for chip in grid.line:
-            own(half, chip)
-    own(0, grid.xp)
-    own(1, grid.yp)
-    own(1, grid.xp)
-    own(0, grid.yp)
+            own(half, line.at[level, d], chip)
+    own(0, relayed.at[level, d, 0], grid.xp)
+    own(1, relayed.at[level, d, 1], grid.yp)
+    own(1, rest.at[0], grid.xp)
+    own(0, rest.at[0], grid.yp)
     for half in range(2):
-        own(half, grid.t, away)
+        own(half, rest.at[1], grid.t, away)
 
         @pl.when(home == d)
         def _(half=half):
@@ -269,35 +268,42 @@
     lots = []
     for k in range(half_z):
         inside = low + lax.rem(grid.z - low + half_z + k, half_z)
-        level = jnp.where(grid.z < low, low + k, jnp.where(grid.z >= low + half_z, low + half_z - 1 - k, inside))
-        lots.append((level * 4 + lax.rem(grid.t, 4), level != grid.z))
+        at = jnp.where(grid.z < low, low + k, jnp.where(grid.z >= low + half_z, low + half_z - 1 - k, inside))
+        lots.append((at * 4 + lax.rem(grid.t, 4), at != grid.z))
+
+    def put(block, r, half, recv, chip, far=None):
+        (out if far is None else extra).put(place(block, r, half), place(block, r, half), recv, chip, d, far)
+
+    def plane(lot, far):
+        level = deep(lot)
+        for r in range(2):
+            landed(share(2), line.at[level, r], grid, far)
+            put(lot, r, 0, relayed.at[level, r, 0], grid.xp, far)
+            put(lot, r, 1, relayed.at[level, r, 1], grid.yp, far)
+            put(lot, r, 1, rest.at[0], grid.xp, far)
+            put(lot, r, 0, rest.at[0], grid.yp, far)
 
     def relay(lot):
-        across, along = grid.over(lot, grid.xp), grid.over(lot, grid.yp)
+        across, along, level = grid.over(lot, grid.xp), grid.over(lot, grid.yp), deep(lot)
         for r in range(2):
-            got(across, r, 0)
-            put(across, r, 0, grid.yp)
-            got(along, r, 1)
-            put(along, r, 1, grid.xp)
+            landed(place(across, r, 0), relayed.at[level, r, 0], grid)
+            put(across, r, 0, rest.at[0], grid.yp)
+            landed(place(along, r, 1), relayed.at[level, r, 1], grid)
+            put(along, r, 1, rest.at[0], grid.xp)
 
     for lot, far in lots:
-        for r in range(2):
-            for half in range(2):
-                got(lot, r, half, far)
-            put(lot, r, 0, grid.xp, far)
-            put(lot, r, 1, grid.yp, far)
-            put(lot, r, 1, grid.xp, far)
-            put(lot, r, 0, grid.yp, far)
+        plane(lot, far)
         relay(lot)
+    landed(share(8 * half_z), rest.at[0], grid)
+    landed(share(2), rest.at[1], grid, home_is(grid))
+    left(share(2 * (grid.nz - 1) + 4 + 4 * half_z), send.at[0], grid)
+    left(share(2), send.at[1], grid, away)
     for lot, far in lots:
-        across, along, corner = grid.over(lot, grid.xp), grid.over(lot, grid.yp), grid.over(lot, grid.xyp)
-        for r in range(2):
-            for half in range(2):
-                got(lot, r, half, jnp.logical_and(jnp.logical_not(far), r != d))
-            got(across, r, 1)
-            got(along, r, 0)
-            got(corner, r, 0)
-            got(corner, r, 1)
+        left(share(8), send.at[1], grid, far)
+
+
+def home_is(grid):
+    return grid.t // grid.per == grid.d
 
 
 def iota(shape, axis):
@@ -353,7 +359,8 @@
 def whole_kernel(
     tp, tok, gain, wr, wk, wv, wd, wa, wg, wo, base_in, ggain_in, state, final, new,
     tokv, w0, w1, gains, part, inbox, acc, near, outw, we, mg, xg, tile, old, terms, reads, proj, base, ggain,
-    load, pair_send, pair_recv, a2a_send, a2a_recv, on_send, on_recv, m_send, m_recv, x_send, x_recv, f_send, f_recv,
+    load, pair_send, pair_recv, a2a_send, a2a_recv, on_send, on_recv, m_send, m_line, m_plane,
+    x_send, x_line, x_relayed, x_rest, f_send, f_line, f_relayed, f_rest,
 ):
     grid = Grid(tp)
     t, d, per = grid.t, grid.d, grid.per
@@ -371,9 +378,9 @@
     get_here = copy(tok.at[pl.ds(here, mine)], tokv.at[pl.ds(here, mine)], 1)
     get_gain = copy(gain, gains.at[d], 2)
     get_base, get_ggain = copy(base_in, base, 3), copy(ggain_in, ggain, 4)
-    get_w0 = [copy(w.at[0], w0.at[pl.ds(i * HEAD, HEAD)], 5 + i) for i, w in enumerate(weights)]
-    get_w1 = [copy(w.at[1], w1.at[d, pl.ds(i * HEAD, HEAD)], 11 + i) for i, w in enumerate(weights)]
-    get_state = [copy(state.at[k], old.at[k], 17 + k) for k in range(LAYERS)]
+    get_w0 = [copy(w.at[0], w0.at[pl.ds(i * HEAD, HEAD)], 5) for i, w in enumerate(weights)]
+    get_w1 = [copy(w.at[1], w1.at[d, pl.ds(i * HEAD, HEAD)], 6) for i, w in enumerate(weights)]
+    get_state = [copy(state.at[k], old.at[k], 7 + k) for k in range(LAYERS)]
     for op in [get_there, get_gain] + get_w0 + [get_here, get_base, get_ggain]:
         op.start()
 
@@ -391,36 +398,41 @@
         normed = (floats * gains[d, 0:1, :]).astype(jnp.bfloat16)
         part[pl.ds(begin, mine), 0:width] = lax.dot_general(normed, w0[...], NT, preferred_element_type=jnp.float32)
 
-    for op in [get_there, get_gain] + get_w0:
-        op.wait()
+    get_there.wait()
+    get_gain.wait()
+    copy(w0, w0, 5).wait()
     project(there)
     pl.semaphore_wait(barrier, 2 * tp - 1)
 
-    pair = Sender(pair_send)
-    pair.put(part.at[pl.ds(there, mine)], inbox, pair_recv.at[0], t, 1 - d)
+    def to_partner(number, src, dst):
+        Sender(pair_send.at[number]).put(src, dst, pair_recv.at[number], t, 1 - d)
+
     slot = lax.rem(t, per)
     slot_cols = pl.ds(pl.multiple_of(slot * cols, cols), cols)
-    pair.put(tokv.at[pl.ds(there, mine), slot_cols], near, pair_recv.at[1], t, 1 - d)
-    pair.put(gains.at[d], gains.at[d], pair_recv.at[2], t, 1 - d)
-
-    a2a = [Sender(a2a_send.at[k]) for k in range(LAYERS)]
-    home = t // per == d
+    to_partner(0, part.at[pl.ds(there, mine)], inbox)
+    to_partner(1, tokv.at[pl.ds(there, mine), slot_cols], near)
+    to_partner(2, gains.at[d], gains.at[d])
+
+    home = home_is(grid)
 
     def spread_weights(layer):
         for c in range(per):
             block = wo.at[layer, :, pl.ds(c * cols, cols)]
             target = d * per + c
-            a2a[layer].put(block, outw.at[layer, t], a2a_recv.at[layer, t], target, d, when=target != t)
+            Sender(a2a_send.at[layer]).put(block, outw.at[layer, t], a2a_recv.at[layer], target, d, when=target != t)
 
             @pl.when(target == t)
             def _(block=block):
-                pltpu.make_async_copy(block, outw.at[layer, t], a2a_recv.at[layer, t]).start()
+                pltpu.make_async_copy(block, outw.at[layer, t], a2a_recv.at[layer]).start()
+
+    def weights_left(layer):
+        left(outw.at[layer, 0:per], a2a_send.at[layer], grid, jnp.logical_not(home))
+        left(outw.at[layer, 0 : per - 1], a2a_send.at[layer], grid, home)
+        left(outw.at[layer], on_send.at[layer], grid, home)
 
     spread_weights(0)
     for i, w in enumerate(weights):
-        block = w1.at[d, pl.ds(i * HEAD, HEAD)]
-        pair.put(w.at[1], block, pair_recv.at[3 + i], t, 1 - d)
-    spread_weights(1)
+        to_partner(3, w.at[1], w1.at[d, pl.ds(i * HEAD, HEAD)])
 
     get_here.wait()
     project(here)
@@ -436,30 +448,14 @@
     ours = home.astype(jnp.float32)
     current = own * ours + near[...].astype(jnp.float32) * (1.0 - ours)
 
-    forwards = [Sender(on_send.at[k]) for k in range(LAYERS)]
-
     def forward_weights(layer):
-        for k in range(tp):
-            source = lax.rem(t + k, tp)
-            block, arrived, onward = outw.at[layer, source], a2a_recv.at[layer, source], on_recv.at[layer, source]
-            if k == 0:
-                @pl.when(home)
-                def _(block=block, arrived=arrived):
-                    pltpu.make_async_copy(block, block, arrived).wait()
-            else:
-                @pl.when(home)
-                def _(block=block, arrived=arrived):
-                    landed(block, arrived, grid)
-            forwards[layer].put(block, block, onward, t, 1 - d, when=home)
-        for k in range(tp):
-            @pl.when(jnp.logical_not(home))
-            def _(k=k):
-                landed(outw.at[layer, k], on_recv.at[layer, k], grid)
+        landed(outw.at[layer], a2a_recv.at[layer], grid, home)
+        Sender(on_send.at[layer]).put(outw.at[layer], outw.at[layer], on_recv.at[layer], t, 1 - d, when=home)
+        landed(outw.at[layer], on_recv.at[layer], grid, jnp.logical_not(home))
 
     def project_out(layer, mixed, current):
         half = mine // 2
         mg[layer, t] = jnp.concatenate([mixed[0:half, :], mixed[half:mine, :]], axis=1)
-        heads = Sender(m_send.at[layer])
 
         def beside():
             forward_weights(layer)
@@ -472,11 +468,10 @@
                 we[bottom, 0:cols] = zero
                 we[bottom, cols : 2 * cols] = block
 
-        gather_heads(grid, mg.at[layer], heads, m_recv.at[layer], beside)
+        gather_heads(grid, mg.at[layer], m_send.at[layer], m_line.at[layer], m_plane.at[layer], beside)
         packed = jnp.concatenate([mg[layer, j] for j in range(tp)], axis=1)
         out = jnp.dot(packed, we[...], preferred_element_type=jnp.float32)
         out = jnp.concatenate([out[:, :cols], out[:, cols:]], axis=0)
-        heads.drain()
         return (current + out).astype(jnp.bfloat16)
 
     seqs = min(mine, 16)
@@ -487,10 +482,8 @@
     lane = cols // 2
     for k in range(2):
         xg[t, k] = stream[:, k * lane : (k + 1) * lane]
-    for op in get_w1:
-        op.wait()
-    for i in range(6):
-        landed(w1.at[1 - d, pl.ds(i * HEAD, HEAD)], pair_recv.at[3 + i], grid)
+    copy(w1.at[d], w1.at[d], 6).wait()
+    landed(w1.at[1 - d], pair_recv.at[3], grid)
     landed(gains.at[1 - d], pair_recv.at[2], grid)
     acc[...] = jnp.zeros(acc.shape, jnp.float32)
 
@@ -504,8 +497,10 @@
         for k in range(cols // PAIR):
             acc[:, width:] += squares[:, k * PAIR : (k + 1) * PAIR]
 
-    tiles = Sender(x_send)
-    gather_tiles(grid, xg, tiles, x_recv, use)
+    def later():
+        spread_weights(1)
+
+    tiles_left = gather_tiles(grid, xg, x_send, x_line, x_relayed, x_rest, later, use)
     inv = lax.rsqrt(jnp.sum(acc[:, width:], axis=1, keepdims=True) / (feats * 2) + norm_floor)
     proj[...] = (inv * acc[:, 0:width]).astype(jnp.bfloat16)
 
@@ -514,11 +509,15 @@
     stream = project_out(1, mixed, stream.astype(jnp.float32))
     for k in range(2):
         tile[k] = stream[:, k * lane : (k + 1) * lane]
-    finish = Sender(f_send)
-    spread_result(grid, tile, final, finish, f_recv)
-
-    for sender in [pair, tiles, finish] + a2a + forwards:
-        sender.drain()
+    spread_result(grid, tile, final, f_send, f_line, f_relayed, f_rest)
+
+    tiles_left()
+    left(part.at[pl.ds(there, mine)], pair_send.at[0], grid)
+    left(near, pair_send.at[1], grid)
+    left(gains.at[d], pair_send.at[2], grid)
+    left(w1.at[d], pair_send.at[3], grid)
+    for layer in range(LAYERS):
+        weights_left(layer)
 
 
 def store_kernel(final, new, final_out, new_out, sems):
@@ -554,8 +553,10 @@
             vmem((tp, 2, mine, cols // 2), bf), vmem((2, mine, cols // 2), bf), vmem(flat.shape, f32),
             vmem((5, mine, PAIR), f32), vmem((mine, PAIR), f32), vmem((mine, width), bf),
             vmem((LAYERS, HEAD), f32), vmem((LAYERS, HEAD), f32),
-            dma((19,)), dma((9,)), dma((9,)), dma((LAYERS, per)), dma((LAYERS, tp)), dma((LAYERS, tp)), dma((LAYERS, tp)),
-            dma((LAYERS, 4 * tp)), dma((LAYERS, tp)), dma((8 * tp,)), dma((tp, 2)), dma((8 * tp,)), dma((per, 2, 2)),
+            dma((9,)), dma((4,)), dma((4,)), dma((LAYERS,)), dma((LAYERS,)), dma((LAYERS,)), dma((LAYERS,)),
+            dma((LAYERS,)), dma((LAYERS, tp // 4)), dma((LAYERS,)),
+            dma, dma((tp // 4,)), dma((tp // 4, 2)), dma((tp // 4,)),
+            dma((2,)), dma((tp // 8, 2)), dma((tp // 8, 2, 2)), dma((2,)),
         ],
         compiler_params=pltpu.CompilerParams(collective_id=0, has_side_effects=True, vmem_limit_bytes=VMEM_LIMIT),
         name="whole",

time: 74.5 us -> 68.6 us (0.921); the launches traced: 74.3 us -> 67.5 us
  Pallas kernels: 73.7 us -> 66.8 us
    pallas_call x1, Pallas kernels: 71.3 us -> 64.4 us  [fast(): pl.pallas_call(functools.partial(whole_kernel, tp), out_shape=(vmem((rows...]
where the time goes in v2:
time: 68.6 us; the launch traced here: 67.5 us
  Pallas kernels  66.8 us (97%)
    pallas_call x1, Pallas kernels, fast(): pl.pallas_call(functools.partial(whole_kernel, tp), out_shape=(vmem((rows...  64.4 us
    pallas_call x1, Pallas kernels, fast(): pl.pallas_call(store_kernel, out_shape=outs, in_specs=[inside, inside], o...  2.37 us

profile of v2, /device:TPU:1, one launch (start us, length us, event | category | flops | bytes accessed | tf_op | source)
XLA Modules:
  0.0 67.5 jit_solution(13842133877131162482)
XLA Ops:
  0.6 64.4 %whole.1 = (bf16[256,2048]{1,0:T(8,128)(2,1)S(1)}, f32[2,4096,128]{2,1,0:T(8,128)S(1)}) custom-call(bf16[256,2048]{1,0:T(8,128)(2,1)} %tok.1, f32[2,2048]{1,0:T(2,128)} %gain.1, bf16[2,64,2048]{2,1,0:T(8,128)(2,1)} %bitcast.9, bf16[2,64,2048]{2,1,0:T(8,128)(2,1)} %bitcast.10, bf16[2,64,2048]{2,1,0:T(8,128)(2,1)} %bitcast.11, bf16[2,64,2048]{2,1,0:T(8,128)(2,1)} %bitcast.12, ...), custom_call_target="tpu_custom_call" | custom-call | tf_op jit(solution)/shard_map/whole/pallas_call | solution.py:543
  65.1 2.4 %store.1 = (bf16[256,2048]{1,0:T(8,128)(2,1)}, f32[2,4096,128]{2,1,0:T(8,128)}) custom-call(bf16[256,2048]{1,0:T(8,128)(2,1)S(1)} %get-tuple-element.6.final, f32[2,4096,128]{2,1,0:T(8,128)S(1)} %get-tuple-element.7.new), custom_call_target="tpu_custom_call" | custom-call | tf_op jit(solution)/shard_map/store/pallas_call | solution.py:564

commit v3 on v2

--- a/solution.py
+++ b/solution.py
@@ -171,22 +171,23 @@
         pl.when(when)(op.wait_send)
 
 
-def gather_heads(grid, buf, send, line, plane, beside):
+def gather_heads(grid, buf, send, line, plane, meanwhile, beside):
     out = Sender(send)
     for chip in grid.line[::-1]:
         out.put(buf.at[grid.t], buf.at[grid.t], line.at[grid.z], chip, grid.d)
     for chip in (grid.xyp, grid.xp, grid.yp):
         out.put(buf.at[grid.t], buf.at[grid.t], plane, chip, grid.d)
-    beside()
+    meanwhile()
     for block in grid.line:
         landed(buf.at[block], line.at[block // 4], grid)
         for chip in (grid.xyp, grid.xp, grid.yp):
             out.put(buf.at[block], buf.at[block], plane, chip, grid.d)
+    beside()
     landed(buf.at[0 : 3 * grid.nz], plane, grid)
     left(buf.at[0 : 4 * grid.nz - 1], send, grid)
 
 
-def gather_tiles(grid, buf, send, line, relayed, rest, after, use):
+def gather_tiles(grid, buf, send, line, relayed, rest, use, after):
     out = Sender(send)
 
     def put(block, half, recv, chip):
@@ -206,20 +207,23 @@
         landed(buf.at[along, 1], relayed.at[level, 1], grid)
         put(along, 1, rest.at[level], grid.xp)
 
-    for half in range(2):
-        for chip in grid.line:
-            put(grid.t, half, line.at[grid.z], chip)
+    for chip in grid.line:
+        out.put(buf.at[grid.t], buf.at[grid.t], line.at[grid.z], chip, grid.d)
     plane(grid.t)
     last = grid.t
-    for block in grid.line:
+    for block in grid.line[:-1]:
         landed(buf.at[block], line.at[block // 4], grid)
         plane(block)
         relay(last)
         last = block
+    block = grid.line[-1]
+    landed(buf.at[block], line.at[block // 4], grid)
+    for chip in (grid.xyp, grid.xp, grid.yp):
+        out.put(buf.at[block], buf.at[block], rest.at[block // 4], chip, grid.d)
     relay(last)
     after()
-    for lot in grid.lots():
-        landed(buf.at[0:2], rest.at[lot // 4], grid)
+    for k, lot in enumerate(grid.lots()):
+        landed(buf.at[0 : 3 if k == grid.nz - 1 else 2], rest.at[lot // 4], grid)
         for block in (lot, grid.over(lot, grid.xp), grid.over(lot, grid.yp), grid.over(lot, grid.xyp)):
             use(block)
 
@@ -291,14 +295,24 @@
             landed(place(along, r, 1), relayed.at[level, r, 1], grid)
             put(along, r, 1, rest.at[0], grid.xp)
 
-    for lot, far in lots:
+    def direct(lot):
+        at = pl.multiple_of(lax.rem(lot, per) * 2 * lane, 2 * lane)
+        for r in range(2):
+            landed(share(2), line.at[deep(lot), r], grid)
+            ref = final.at[pl.ds(r * rows, rows), pl.ds(at, 2 * lane)]
+            for chip in (grid.xyp, grid.xp, grid.yp):
+                out.put(ref, ref, rest.at[0], chip, d)
+
+    for lot, far in lots[:-1]:
         plane(lot, far)
+    direct(lots[-1][0])
+    for lot, far in lots[:-1]:
         relay(lot)
-    landed(share(8 * half_z), rest.at[0], grid)
+    landed(share(8 * half_z + 4), rest.at[0], grid)
     landed(share(2), rest.at[1], grid, home_is(grid))
-    left(share(2 * (grid.nz - 1) + 4 + 4 * half_z), send.at[0], grid)
+    left(share(2 * (grid.nz - 1) + 4 * half_z + 12), send.at[0], grid)
     left(share(2), send.at[1], grid, away)
-    for lot, far in lots:
+    for lot, far in lots[:-1]:
         left(share(8), send.at[1], grid, far)
 
 
@@ -402,6 +416,8 @@
     get_gain.wait()
     copy(w0, w0, 5).wait()
     project(there)
+    get_here.wait()
+    project(here)
     pl.semaphore_wait(barrier, 2 * tp - 1)
 
     def to_partner(number, src, dst):
@@ -434,8 +450,6 @@
     for i, w in enumerate(weights):
         to_partner(3, w.at[1], w1.at[d, pl.ds(i * HEAD, HEAD)])
 
-    get_here.wait()
-    project(here)
     get_base.wait()
     get_ggain.wait()
     landed(inbox, pair_recv.at[0], grid)
@@ -456,6 +470,10 @@
     def project_out(layer, mixed, current):
         half = mine // 2
         mg[layer, t] = jnp.concatenate([mixed[0:half, :], mixed[half:mine, :]], axis=1)
+
+        def meanwhile():
+            if layer + 1 < LAYERS:
+                pass
 
         def beside():
             forward_weights(layer)
@@ -468,7 +486,7 @@
                 we[bottom, 0:cols] = zero
                 we[bottom, cols : 2 * cols] = block
 
-        gather_heads(grid, mg.at[layer], m_send.at[layer], m_line.at[layer], m_plane.at[layer], beside)
+        gather_heads(grid, mg.at[layer], m_send.at[layer], m_line.at[layer], m_plane.at[layer], meanwhile, beside)
         packed = jnp.concatenate([mg[layer, j] for j in range(tp)], axis=1)
         out = jnp.dot(packed, we[...], preferred_element_type=jnp.float32)
         out = jnp.concatenate([out[:, :cols], out[:, cols:]], axis=0)
@@ -497,10 +515,7 @@
         for k in range(cols // PAIR):
             acc[:, width:] += squares[:, k * PAIR : (k + 1) * PAIR]
 
-    def later():
-        spread_weights(1)
-
-    tiles_left = gather_tiles(grid, xg, x_send, x_line, x_relayed, x_rest, later, use)
+    tiles_left = gather_tiles(grid, xg, x_send, x_line, x_relayed, x_rest, use, lambda: spread_weights(1))
     inv = lax.rsqrt(jnp.sum(acc[:, width:], axis=1, keepdims=True) / (feats * 2) + norm_floor)
     proj[...] = (inv * acc[:, 0:width]).astype(jnp.bfloat16)
 
@@ -576,7 +591,7 @@
 def step(tp, dp, tokens, norm_gain, *rest):
     projections, (decay_base, group_gain, output_proj, state) = rest[:6], rest[6:]
     rows, feats = tokens.shape
-    fits = dp == 2 and tp % 8 == 0 and state.shape[2] == 1 and state.shape[1] % 64 == 0 and (feats * dp // tp) % 256 == 0
+    fits = dp == 2 and tp % 16 == 0 and state.shape[2] == 1 and state.shape[1] % 64 == 0 and (feats * dp // tp) % 256 == 0
     if fits:
         return fast(tp, tokens, norm_gain, projections, decay_base, group_gain, output_proj, state)
     return shards(tokens, norm_gain, *rest)

time: 68.6 us -> 65.4 us (0.953); the launches traced: 67.5 us -> 65.2 us
  Pallas kernels: 66.8 us -> 64.6 us
    pallas_call x1, Pallas kernels: 64.4 us -> 62.2 us  [fast(): pl.pallas_call(functools.partial(whole_kernel, tp), out_shape=(vmem((rows...]
where the time goes in v3:
time: 65.4 us; the launch traced here: 65.2 us
  Pallas kernels  64.6 us (99%)
    pallas_call x1, Pallas kernels, fast(): pl.pallas_call(functools.partial(whole_kernel, tp), out_shape=(vmem((rows...  62.2 us
    pallas_call x1, Pallas kernels, fast(): pl.pallas_call(store_kernel, out_shape=outs, in_specs=[inside, inside], o...  2.37 us

profile of v3, /device:TPU:1, one launch (start us, length us, event | category | flops | bytes accessed | tf_op | source)
XLA Modules:
  0.0 65.2 jit_solution(17324698868741617298)
XLA Ops:
  0.6 62.2 %whole.1 = (bf16[256,2048]{1,0:T(8,128)(2,1)S(1)}, f32[2,4096,128]{2,1,0:T(8,128)S(1)}) custom-call(bf16[256,2048]{1,0:T(8,128)(2,1)} %tok.1, f32[2,2048]{1,0:T(2,128)} %gain.1, bf16[2,64,2048]{2,1,0:T(8,128)(2,1)} %bitcast.9, bf16[2,64,2048]{2,1,0:T(8,128)(2,1)} %bitcast.10, bf16[2,64,2048]{2,1,0:T(8,128)(2,1)} %bitcast.11, bf16[2,64,2048]{2,1,0:T(8,128)(2,1)} %bitcast.12, ...), custom_call_target="tpu_custom_call" | custom-call | tf_op jit(solution)/shard_map/whole/pallas_call | solution.py:558
  62.9 2.4 %store.1 = (bf16[256,2048]{1,0:T(8,128)(2,1)}, f32[2,4096,128]{2,1,0:T(8,128)}) custom-call(bf16[256,2048]{1,0:T(8,128)(2,1)S(1)} %get-tuple-element.6.final, f32[2,4096,128]{2,1,0:T(8,128)S(1)} %get-tuple-element.7.new), custom_call_target="tpu_custom_call" | custom-call | tf_op jit(solution)/shard_map/store/pallas_call | solution.py:579

commit v4 on v3

--- a/solution.py
+++ b/solution.py
@@ -1,4 +1,5 @@
 import functools
+import math
 
 import jax
 import jax.numpy as jnp
@@ -324,19 +325,23 @@
     return lax.broadcasted_iota(jnp.int32, shape, axis)
 
 
-def update_state(proj, base, ggain, layer, old, new, terms, reads, seqs):
+def update_state(proj, base, ggain, layer, old, new, terms, reads, doubled, seqs):
     mine = proj.shape[0]
     lines = old.shape[1] // mine
+    wide = jnp.dot(proj[...], doubled[...], preferred_element_type=jnp.float32)
 
     def piece(i):
-        return proj[:, i * HEAD : (i + 1) * HEAD].astype(jnp.float32)
-
-    recept, key, value, decay, rate = [piece(i) for i in range(5)]
-    scale = lax.rsqrt(jnp.sum(key * key, axis=-1, keepdims=True) + 1.0)
-    forget = jnp.exp(-jnp.exp(-jax.nn.softplus(-(decay + base[layer : layer + 1, :])) - 0.5))
+        return wide[:, i * PAIR : (i + 1) * PAIR]
+
+    def twice(row):
+        return jnp.concatenate([row, row], axis=-1)
+
+    recept, key, value, decay, rate, gate = [piece(i) for i in range(6)]
+    scale = lax.rsqrt(jnp.sum(key * key, axis=-1, keepdims=True) * 0.5 + 1.0)
+    forget = jnp.exp(-math.exp(-0.5) * jax.nn.sigmoid(decay + twice(base[layer : layer + 1, :])))
     learned = key * jax.nn.sigmoid(rate)
     for i, term in enumerate((key * (-scale * scale), forget, learned, recept, value)):
-        terms[i] = jnp.concatenate([term, term], axis=-1)
+        terms[i] = term
 
     lane, col = iota((PAIR, PAIR), 0), iota((PAIR, PAIR), 1)
     same = (lane // HEAD == col // HEAD).astype(jnp.bfloat16)
@@ -364,16 +369,18 @@
         return carry
 
     lax.fori_loop(0, mine // seqs, step, 0)
-    read = reads[:, :HEAD]
+    read = reads[...]
     centre = read - jnp.mean(read, axis=-1, keepdims=True)
     normal = centre * lax.rsqrt(jnp.mean(centre * centre, axis=-1, keepdims=True) + group_floor)
-    return (normal * ggain[layer : layer + 1, :] * jax.nn.sigmoid(piece(5))).astype(jnp.bfloat16)
+    mixed = normal * twice(ggain[layer : layer + 1, :]) * jax.nn.sigmoid(gate)
+    first = iota((mine // 2, PAIR), 1) < HEAD
+    return jnp.where(first, mixed[0 : mine // 2], mixed[mine // 2 : mine]).astype(jnp.bfloat16)
 
 
 def whole_kernel(
     tp, tok, gain, wr, wk, wv, wd, wa, wg, wo, base_in, ggain_in, state, final, new,
-    tokv, w0, w1, gains, part, inbox, acc, near, outw, we, mg, xg, tile, old, terms, reads, proj, base, ggain,
-    load, pair_send, pair_recv, a2a_send, a2a_recv, on_send, on_recv, m_send, m_line, m_plane,
+    tokv, w0, w1, gains, part, inbox, acc, near, outw, wov, hub, we, mg, xg, tile, old, terms, reads, doubled, proj, base, ggain,
+    load, pair_send, pair_recv, hub_send, hub_recv, a2a_send, a2a_recv, on_send, on_recv, m_send, m_line, m_plane,
     x_send, x_line, x_relayed, x_rest, f_send, f_line, f_relayed, f_rest,
 ):
     grid = Grid(tp)
@@ -394,6 +401,7 @@
     get_base, get_ggain = copy(base_in, base, 3), copy(ggain_in, ggain, 4)
     get_w0 = [copy(w.at[0], w0.at[pl.ds(i * HEAD, HEAD)], 5) for i, w in enumerate(weights)]
     get_w1 = [copy(w.at[1], w1.at[d, pl.ds(i * HEAD, HEAD)], 6) for i, w in enumerate(weights)]
+    get_wo = copy(wo.at[0], wov, 9)
     get_state = [copy(state.at[k], old.at[k], 7 + k) for k in range(LAYERS)]
     for op in [get_there, get_gain] + get_w0 + [get_here, get_base, get_ggain]:
         op.start()
@@ -403,8 +411,11 @@
         for core in range(2):
             pl.semaphore_signal(barrier, inc=1, device_id={"tp": lax.rem(t + k, tp), "dp": core}, device_id_type=MESH)
     pl.semaphore_signal(barrier, inc=1, device_id={"tp": t, "dp": 1 - d}, device_id_type=MESH)
-    for op in [get_state[0]] + get_w1 + [get_state[1]]:
+    for op in [get_wo, get_state[0]] + get_w1 + [get_state[1]]:
         op.start()
+    source, column = iota((width, 2 * width), 0), iota((width, 2 * width), 1)
+    wanted = column // PAIR * HEAD + column % HEAD
+    doubled[...] = (source == wanted).astype(jnp.bfloat16)
 
     def project(begin):
         floats = tokv[pl.ds(begin, mine), :].astype(jnp.float32)
@@ -431,22 +442,52 @@
 
     home = home_is(grid)
 
-    def spread_weights(layer):
+    def spread_weights():
         for c in range(per):
-            block = wo.at[layer, :, pl.ds(c * cols, cols)]
+            block = wov.at[:, pl.ds(c * cols, cols)]
             target = d * per + c
-            Sender(a2a_send.at[layer]).put(block, outw.at[layer, t], a2a_recv.at[layer], target, d, when=target != t)
+            Sender(a2a_send.at[0]).put(block, outw.at[0, t], a2a_recv.at[0], target, d, when=target != t)
 
             @pl.when(target == t)
+            def _(c=c):
+                outw[0, t] = wov[:, c * cols : (c + 1) * cols]
+
+    half_z = grid.nz // 2
+
+    def spread_planes():
+        for k in range(half_z):
+            block = wo.at[1, :, pl.ds(k * 4 * cols, 4 * cols)]
+            level = d * half_z + k
+            Sender(hub_send).put(block, hub.at[grid.z], hub_recv, level * 4 + lax.rem(t, 4), d, when=level != grid.z)
+
+            @pl.when(level == grid.z)
             def _(block=block):
-                pltpu.make_async_copy(block, outw.at[layer, t], a2a_recv.at[layer]).start()
-
-    def weights_left(layer):
-        left(outw.at[layer, 0:per], a2a_send.at[layer], grid, jnp.logical_not(home))
-        left(outw.at[layer, 0 : per - 1], a2a_send.at[layer], grid, home)
-        left(outw.at[layer], on_send.at[layer], grid, home)
-
-    spread_weights(0)
+                pltpu.make_async_copy(block, hub.at[grid.z], hub_recv).start()
+
+    def spread_plane():
+        landed(hub, hub_recv, grid, home)
+        for level in range(grid.nz):
+            source = level * 4 + lax.rem(t, 4)
+            for chip in (grid.xyp, grid.xp, grid.yp):
+                block = hub.at[level, :, pl.ds(pl.multiple_of(lax.rem(chip, 4) * cols, cols), cols)]
+                Sender(a2a_send.at[1]).put(block, outw.at[1, source], a2a_recv.at[1], chip, d, when=home)
+
+            @pl.when(home)
+            def _(level=level, source=source):
+                outw[1, source] = hub[level, :, pl.ds(pl.multiple_of(lax.rem(t, 4) * cols, cols), cols)]
+
+    def weights_left():
+        away = jnp.logical_not(home)
+        left(outw.at[0, 0:per], a2a_send.at[0], grid, away)
+        left(outw.at[0, 0 : per - 1], a2a_send.at[0], grid, home)
+        left(hub.at[0:half_z], hub_send, grid, away)
+        left(hub.at[0 : half_z - 1], hub_send, grid, home)
+        left(outw.at[1, 0 : 3 * grid.nz], a2a_send.at[1], grid, home)
+        for layer in range(LAYERS):
+            left(outw.at[layer], on_send.at[layer], grid, home)
+
+    get_wo.wait()
+    spread_weights()
     for i, w in enumerate(weights):
         to_partner(3, w.at[1], w1.at[d, pl.ds(i * HEAD, HEAD)])
 
@@ -463,20 +504,21 @@
     current = own * ours + near[...].astype(jnp.float32) * (1.0 - ours)
 
     def forward_weights(layer):
-        landed(outw.at[layer], a2a_recv.at[layer], grid, home)
+        landed(outw.at[layer, 0 : (tp - 1 if layer == 0 else 3 * grid.nz)], a2a_recv.at[layer], grid, home)
         Sender(on_send.at[layer]).put(outw.at[layer], outw.at[layer], on_recv.at[layer], t, 1 - d, when=home)
         landed(outw.at[layer], on_recv.at[layer], grid, jnp.logical_not(home))
 
     def project_out(layer, mixed, current):
-        half = mine // 2
-        mg[layer, t] = jnp.concatenate([mixed[0:half, :], mixed[half:mine, :]], axis=1)
+        mg[layer, t] = mixed
 
         def meanwhile():
-            if layer + 1 < LAYERS:
-                pass
+            if layer == 0:
+                spread_planes()
 
         def beside():
-            forward_weights(layer)
+            if layer == 0:
+                forward_weights(0)
+                spread_plane()
             zero = jnp.zeros((HEAD, cols), we.dtype)
             for k in range(tp):
                 block = outw[layer, k]
@@ -492,9 +534,9 @@
         out = jnp.concatenate([out[:, :cols], out[:, cols:]], axis=0)
         return (current + out).astype(jnp.bfloat16)
 
-    seqs = min(mine, 16)
+    seqs = min(mine, 64)
     get_state[0].wait()
-    mixed = update_state(proj, base, ggain, 0, old, new, terms, reads, seqs)
+    mixed = update_state(proj, base, ggain, 0, old, new, terms, reads, doubled, seqs)
     stream = project_out(0, mixed, current)
 
     lane = cols // 2
@@ -515,12 +557,12 @@
         for k in range(cols // PAIR):
             acc[:, width:] += squares[:, k * PAIR : (k + 1) * PAIR]
 
-    tiles_left = gather_tiles(grid, xg, x_send, x_line, x_relayed, x_rest, use, lambda: spread_weights(1))
+    tiles_left = gather_tiles(grid, xg, x_send, x_line, x_relayed, x_rest, use, lambda: forward_weights(1))
     inv = lax.rsqrt(jnp.sum(acc[:, width:], axis=1, keepdims=True) / (feats * 2) + norm_floor)
     proj[...] = (inv * acc[:, 0:width]).astype(jnp.bfloat16)
 
     get_state[1].wait()
-    mixed = update_state(proj, base, ggain, 1, old, new, terms, reads, seqs)
+    mixed = update_state(proj, base, ggain, 1, old, new, terms, reads, doubled, seqs)
     stream = project_out(1, mixed, stream.astype(jnp.float32))
     for k in range(2):
         tile[k] = stream[:, k * lane : (k + 1) * lane]
@@ -531,8 +573,7 @@
     left(near, pair_send.at[1], grid)
     left(gains.at[d], pair_send.at[2], grid)
     left(w1.at[d], pair_send.at[3], grid)
-    for layer in range(LAYERS):
-        weights_left(layer)
+    weights_left()
 
 
 def store_kernel(final, new, final_out, new_out, sems):
@@ -564,11 +605,12 @@
             vmem((rows, feats), bf), vmem((width, feats), bf), vmem((2, width, feats), bf), vmem((2, LAYERS, feats), f32),
             vmem((rows, width + PAIR), f32), vmem((mine, width + PAIR), f32), vmem((mine, width + PAIR), f32),
             vmem((mine, cols), bf),
-            vmem((LAYERS, tp, HEAD, cols), bf), vmem((tp * PAIR, 2 * cols), bf), vmem((LAYERS, tp, mine // 2, PAIR), bf),
+            vmem((LAYERS, tp, HEAD, cols), bf), vmem((HEAD, feats), bf), vmem((tp // 4, HEAD, 4 * cols), bf), vmem((tp * PAIR, 2 * cols), bf), vmem((LAYERS, tp, mine // 2, PAIR), bf),
             vmem((tp, 2, mine, cols // 2), bf), vmem((2, mine, cols // 2), bf), vmem(flat.shape, f32),
-            vmem((5, mine, PAIR), f32), vmem((mine, PAIR), f32), vmem((mine, width), bf),
+            vmem((5, mine, PAIR), f32), vmem((mine, PAIR), f32), vmem((width, 2 * width), bf),
+            vmem((mine, width), bf),
             vmem((LAYERS, HEAD), f32), vmem((LAYERS, HEAD), f32),
-            dma((9,)), dma((4,)), dma((4,)), dma((LAYERS,)), dma((LAYERS,)), dma((LAYERS,)), dma((LAYERS,)),
+            dma((10,)), dma((4,)), dma((4,)), dma, dma, dma((LAYERS,)), dma((LAYERS,)), dma((LAYERS,)), dma((LAYERS,)),
             dma((LAYERS,)), dma((LAYERS, tp // 4)), dma((LAYERS,)),
             dma, dma((tp // 4,)), dma((tp // 4, 2)), dma((tp // 4,)),
             dma((2,)), dma((tp // 8, 2)), dma((tp // 8, 2, 2)), dma((2,)),

time: 65.4 us -> 64.3 us (0.983)
  Pallas kernels: 64.6 us -> 63.5 us
    pallas_call x1, Pallas kernels: 62.2 us -> 61.1 us  [fast(): pl.pallas_call(functools.partial(whole_kernel, tp), out_shape=(vmem((rows...]
where the time goes in v4:
time: 64.3 us; the launch traced here: 64.1 us
  Pallas kernels  63.5 us (99%)
    pallas_call x1, Pallas kernels, fast(): pl.pallas_call(functools.partial(whole_kernel, tp), out_shape=(vmem((rows...  61.1 us
    pallas_call x1, Pallas kernels, fast(): pl.pallas_call(store_kernel, out_shape=outs, in_specs=[inside, inside], o...  2.37 us

profile of v4, /device:TPU:1, one launch (start us, length us, event | category | flops | bytes accessed | tf_op | source)
XLA Modules:
  0.0 64.1 jit_solution(6783999037971297294)
XLA Ops:
  0.6 61.1 %whole.1 = (bf16[256,2048]{1,0:T(8,128)(2,1)S(1)}, f32[2,4096,128]{2,1,0:T(8,128)S(1)}) custom-call(bf16[256,2048]{1,0:T(8,128)(2,1)} %tok.1, f32[2,2048]{1,0:T(2,128)} %gain.1, bf16[2,64,2048]{2,1,0:T(8,128)(2,1)} %bitcast.9, bf16[2,64,2048]{2,1,0:T(8,128)(2,1)} %bitcast.10, bf16[2,64,2048]{2,1,0:T(8,128)(2,1)} %bitcast.11, bf16[2,64,2048]{2,1,0:T(8,128)(2,1)} %bitcast.12, ...), custom_call_target="tpu_custom_call" | custom-call | tf_op jit(solution)/shard_map/whole/pallas_call | solution.py:599
  61.8 2.4 %store.1 = (bf16[256,2048]{1,0:T(8,128)(2,1)}, f32[2,4096,128]{2,1,0:T(8,128)}) custom-call(bf16[256,2048]{1,0:T(8,128)(2,1)S(1)} %get-tuple-element.6.final, f32[2,4096,128]{2,1,0:T(8,128)S(1)} %get-tuple-element.7.new), custom_call_target="tpu_custom_call" | custom-call | tf_op jit(solution)/shard_map/store/pallas_call | solution.py:621

commit v5 on v4

--- a/solution.py
+++ b/solution.py
@@ -506,6 +506,8 @@
     def forward_weights(layer):
         landed(outw.at[layer, 0 : (tp - 1 if layer == 0 else 3 * grid.nz)], a2a_recv.at[layer], grid, home)
         Sender(on_send.at[layer]).put(outw.at[layer], outw.at[layer], on_recv.at[layer], t, 1 - d, when=home)
+
+    def weights_here(layer):
         landed(outw.at[layer], on_recv.at[layer], grid, jnp.logical_not(home))
 
     def project_out(layer, mixed, current):
@@ -519,6 +521,7 @@
             if layer == 0:
                 forward_weights(0)
                 spread_plane()
+            weights_here(layer)
             zero = jnp.zeros((HEAD, cols), we.dtype)
             for k in range(tp):
                 block = outw[layer, k]

time: 64.3 us -> 64 us (level)
  no operation moved by 1% of the time
where the time goes in v5:
time: 64 us; the launch traced here: 63.8 us
  Pallas kernels  63.2 us (99%)
  between operations  0.64 us (1%)
    pallas_call x1, Pallas kernels, fast(): pl.pallas_call(functools.partial(whole_kernel, tp), out_shape=(vmem((rows...  60.8 us
    pallas_call x1, Pallas kernels, fast(): pl.pallas_call(store_kernel, out_shape=outs, in_specs=[inside, inside], o...  2.37 us

profile of v5, /device:TPU:1, one launch (start us, length us, event | category | flops | bytes accessed | tf_op | source)
XLA Modules:
  0.0 63.8 jit_solution(13559295959766119176)
XLA Ops:
  0.6 60.8 %whole.1 = (bf16[256,2048]{1,0:T(8,128)(2,1)S(1)}, f32[2,4096,128]{2,1,0:T(8,128)S(1)}) custom-call(bf16[256,2048]{1,0:T(8,128)(2,1)} %tok.1, f32[2,2048]{1,0:T(2,128)} %gain.1, bf16[2,64,2048]{2,1,0:T(8,128)(2,1)} %bitcast.9, bf16[2,64,2048]{2,1,0:T(8,128)(2,1)} %bitcast.10, bf16[2,64,2048]{2,1,0:T(8,128)(2,1)} %bitcast.11, bf16[2,64,2048]{2,1,0:T(8,128)(2,1)} %bitcast.12, ...), custom_call_target="tpu_custom_call" | custom-call | tf_op jit(solution)/shard_map/whole/pallas_call | solution.py:602
  61.5 2.4 %store.1 = (bf16[256,2048]{1,0:T(8,128)(2,1)}, f32[2,4096,128]{2,1,0:T(8,128)}) custom-call(bf16[256,2048]{1,0:T(8,128)(2,1)S(1)} %get-tuple-element.6.final, f32[2,4096,128]{2,1,0:T(8,128)S(1)} %get-tuple-element.7.new), custom_call_target="tpu_custom_call" | custom-call | tf_op jit(solution)/shard_map/store/pallas_call | solution.py:624
